TPU v7x, 32 devices: a whole 2x2x4 slice. The times are simulated.
32 devices in a mesh: ep: 16 (over z, y, x), tp: 2 (over core).
Axes of the slice: x: 2, y: 2, z: 4, core: 2. Of those that a mesh axis runs over, the one named last changes fastest.
Arguments:
- residual: bfloat16 [1024, 2048], P('ep', 'tp'), may hold values from -100 to 100
- route_ids: int32 [1024, 4], P('ep'), may hold values from 0 to 15, all different within a row; in each aligned block of 64 rows (0 to 63, 64 to 127, ...) at most 24 rows name the same one
- route_weights: float32 [1024, 4], P('ep'), may hold values from 0.1 to 1
- carried_state: float32 [2, 1024, 4096], P(None, 'ep', 'tp'), may hold values from -6 to 6
- mix_gain: float32 [2048], replicated, may hold values from 0.1 to 1.9
- in_proj: bfloat16 [2048, 1024], P(None, 'tp'), may hold values from -0.125 to 0.125
- decay_rate: float32 [64, 64], P('tp'), may hold values from 0.1 to 2
- frequency: float32 [64, 64], P('tp'), may hold values from -3 to 3
- step_size: float32 [64], P('tp'), may hold values from 0.05 to 1
- input_map: float32 [2, 64, 64, 16], P(None, 'tp'), may hold values from -1.5 to 1.5
- output_matrix: float32 [2, 64, 16, 64], P(None, 'tp'), may hold values from -0.5 to 0.5
- passthrough_scale: float32 [1024], P('tp'), may hold values from -4 to 4
- out_gain: float32 [1024], replicated, may hold values from 0.1 to 1.9
- out_proj: bfloat16 [1024, 2048], P(None, 'tp'), may hold values from -0.1875 to 0.1875
- ffn_gain: float32 [2048], replicated, may hold values from 0.1 to 1.9
- w_gate: bfloat16 [16, 2048, 2048], P('ep', None, 'tp'), may hold values from -5 to 5
- w_up: bfloat16 [16, 2048, 2048], P('ep', None, 'tp'), may hold values from -5 to 5
- w_down: bfloat16 [16, 2048, 2048], P('ep', 'tp'), may hold values from -0.125 to 0.125
Outputs:
- updated: bfloat16 [1024, 2048], P('ep', 'tp')
- new_state: float32 [2, 1024, 4096], P(None, 'ep', 'tp')
Inputs may be any that keep to these rules, and one draw needn't show every extreme that they name: `route_ids`: each row names 4 different experts. Among the 64 rows of one device (aligned blocks) no expert is named more than 24 times, and in every draw some block names some expert exactly 24 times.
All inputs are finite; a program needn't handle non-finite values.
Results may differ from a plain program's by a relative error of at most 0.018.
Values may be sent and summed in bfloat16 or wider, within the bound.
No kernel may reach another device: no remote copies, remote signals or barrier semaphores. Data moves between devices by JAX's collectives and lax.ppermute only.
A program may use at most 128 MiB of HBM per device.

v0:
```python
import functools

import jax
import jax.numpy as jnp
from jax import lax
from jax.experimental import pallas as pl
from jax.experimental.pallas import tpu as pltpu
from jax.sharding import PartitionSpec as P


epsilon = 1e-06
clamp_limit = 7.0
swish_alpha = 1.702
f32, bf16 = jnp.float32, jnp.bfloat16
NN = (((1,), (0,)), ((), ()))
NT = (((1,), (1,)), ((), ()))
TN = (((0,), (0,)), ((), ()))
MIXER_VMEM = 16
HEAD_FLOPS = 10**11


def mm(a, b, dims=NN):
    return lax.dot_general(a, b, dims, preferred_element_type=f32)


def split(values):
    high = values.astype(bf16)
    return high, (values - high.astype(f32)).astype(bf16)


def flat_row(table):
    groups, width = table.shape
    tiled = jnp.concatenate([table] * groups, axis=1)
    lane = lax.broadcasted_iota(jnp.int32, tiled.shape, 1)
    first = lax.broadcasted_iota(jnp.int32, tiled.shape, 0) * width
    own = (lane >= first) & (lane < first + width)
    return jnp.sum(jnp.where(own, tiled, 0.0), axis=0, keepdims=True)


def spread(table, count):
    _, per_group, width = table.shape
    tiled = jnp.concatenate([table] * count, axis=2)
    lane = lax.broadcasted_iota(jnp.int32, tiled.shape, 2)
    first = lax.broadcasted_iota(jnp.int32, tiled.shape, 0) * width
    own = (lane >= first) & (lane < first + width)
    return jnp.where(own, tiled, 0.0).reshape(count * per_group, count * width)


def head_kernel(out_ref):
    out_ref[...] = jnp.zeros_like(out_ref)


def mixer_kernel(*refs):
    decay_ref, freq_ref, step_ref, map_ref, out_ref, own_ref, other_ref, gain_ref = refs[:8]
    proj_ref, skip_ref, ids_ref, weights_ref, state_ref, _, act_ref, new_ref = refs[8:]
    groups, width = decay_ref.shape
    per_group = map_ref.shape[2]
    step = step_ref[...]
    square = jnp.broadcast_to(step, (groups, groups))
    diagonal = lax.broadcasted_iota(jnp.int32, square.shape, 0) == lax.broadcasted_iota(
        jnp.int32, square.shape, 1
    )
    step = jnp.sum(jnp.where(diagonal, square, 0.0), axis=1, keepdims=True)
    rate, freq = -decay_ref[...], freq_ref[...]
    magnitude = jnp.exp(rate * step)
    phase = freq * step
    bar_real, bar_imag = magnitude * jnp.cos(phase), magnitude * jnp.sin(phase)
    inverse = 1.0 / (rate * rate + freq * freq)
    shifted = bar_real - 1.0
    coef_real = ((shifted * rate + bar_imag * freq) * inverse)[:, None, :]
    coef_imag = ((bar_imag * rate - shifted * freq) * inverse)[:, None, :]
    map_real = coef_real * map_ref[0] - coef_imag * map_ref[1]
    map_imag = coef_real * map_ref[1] + coef_imag * map_ref[0]
    bar_real, bar_imag = flat_row(bar_real), flat_row(bar_imag)
    count = max(1, min(groups, 128 // per_group))
    blocks = [slice(i * count, (i + 1) * count) for i in range(groups // count)]
    tables = [
        split(spread(map_real[held], count))
        + split(spread(map_imag[held], count))
        + (spread(out_ref[0, held], count).astype(bf16), spread(-out_ref[1, held], count).astype(bf16))
        for held in blocks
    ]
    low, high = normed(own_ref[...], other_ref[...], gain_ref[...], lax.axis_index("tp") == 0)
    half = low.shape[1]
    channels = (mm(low, proj_ref[:half, :]) + mm(high, proj_ref[half:, :])).astype(bf16)
    rows = low.shape[0]
    lanes, columns = count * width, count * per_group
    for block, (real_high, real_low, imag_high, imag_low, out_real, out_imag) in enumerate(tables):
        wide = slice(block * lanes, (block + 1) * lanes)
        narrow = slice(block * columns, (block + 1) * columns)
        fed = channels[:, narrow]
        old_real, old_imag = state_ref[0, :, wide], state_ref[1, :, wide]
        turn_real, turn_imag = bar_real[:, wide], bar_imag[:, wide]
        next_real = (
            turn_real * old_real - turn_imag * old_imag + (mm(fed, real_high) + mm(fed, real_low))
        )
        next_imag = (
            turn_real * old_imag + turn_imag * old_real + (mm(fed, imag_high) + mm(fed, imag_low))
        )
        new_ref[0, :, wide] = next_real
        new_ref[1, :, wide] = next_imag
        mixed = mm(next_real.astype(bf16), out_real, NT) + mm(next_imag.astype(bf16), out_imag, NT)
        mixed = mixed + skip_ref[:, narrow] * fed.astype(f32)
        act_ref[:rows, narrow] = jax.nn.gelu(mixed).astype(bf16)
    weights = weights_ref[...]
    w_high = weights.astype(bf16).astype(f32)
    w_mid = (weights - w_high).astype(bf16).astype(f32)
    w_low = weights - w_high - w_mid
    parts = (ids_ref[...].astype(f32), w_high, w_mid, w_low)
    top = weights.shape[0]
    each = act_ref.shape[1] // rows
    lines = -(-4 * top // each)
    tags = [
        jnp.concatenate(
            [jnp.concatenate(parts, axis=0)[i : i + 1, :] for i in range(4 * top)][k * each : (k + 1) * each],
            axis=1,
        )
        for k in range(lines)
    ]
    tags.append(jnp.zeros((act_ref.shape[0] - rows - lines, act_ref.shape[1]), f32))
    act_ref[rows:, :] = jnp.concatenate(tags, axis=0).astype(bf16)


def normed(own, other, gain, first):
    own, other = own.astype(f32), other.astype(f32)
    half = own.shape[1]
    low, high = jnp.where(first, own, other), jnp.where(first, other, own)
    total = jnp.sum(low * low, axis=1, keepdims=True) + jnp.sum(high * high, axis=1, keepdims=True)
    scale = lax.rsqrt(total / (2 * half) + epsilon)
    return (
        (low * scale * gain[:, :half]).astype(bf16),
        (high * scale * gain[:, half:]).astype(bf16),
    )


def dispatch_kernel(
    chosen,
    span,
    top,
    own_ref,
    other_ref,
    far_own_ref,
    far_other_ref,
    gain_ref,
    proj_ref,
    residual_ref,
    far_residual_ref,
    mid_ref,
    high_ref,
    low_ref,
    *sent_refs,
):
    first = lax.axis_index("tp") == 0
    count = residual_ref.shape[0]
    own = jnp.concatenate([own_ref[:count], far_own_ref[:count]], axis=0)
    other = jnp.concatenate([other_ref[:count], far_other_ref[:count]], axis=0)
    low, high = normed(own, other, gain_ref[...], first)
    half = own.shape[1]
    product = mm(low, proj_ref[:half, :]) + mm(high, proj_ref[half:, :])
    residual = jnp.concatenate([residual_ref[...], far_residual_ref[...]], axis=0)
    mid = (residual.astype(f32) + product).astype(bf16)
    mid_ref[...] = mid[: mid_ref.shape[0]]

    each = half // count
    tags = [ref[count:].astype(f32) for ref in (own_ref, far_own_ref)]
    tags = jnp.concatenate(
        [
            jnp.concatenate(
                [
                    tag[i // each : i // each + 1, i % each * count : (i % each + 1) * count]
                    for i in range(4 * top)
                ],
                axis=0,
            )
            for tag in tags
        ],
        axis=1,
    )
    rows = tags.shape[1]
    ids = tags[:top].astype(jnp.int32)
    weights = tags[top : 2 * top] + tags[2 * top : 3 * top] + tags[3 * top :]
    place = lax.axis_index("ep")
    base = place // chosen * chosen
    turn = lax.broadcasted_iota(jnp.int32, (chosen, rows), 0)
    expert = base + (turn ^ (place - base))
    named = jnp.zeros((chosen, rows), f32)
    weight = jnp.zeros((chosen, rows), f32)
    for k in range(top):
        same = ids[k : k + 1, :] == expert
        named = named + same.astype(f32)
        weight = weight + jnp.where(same, weights[k : k + 1, :], 0.0)
    earlier = lax.broadcasted_iota(jnp.int32, (rows, rows), 0) < lax.broadcasted_iota(
        jnp.int32, (rows, rows), 1
    )
    rank = mm(named.astype(bf16), earlier.astype(f32).astype(bf16))
    rank = jnp.where(named > 0.0, rank, -1.0).astype(jnp.int32)
    slot = lax.broadcasted_iota(jnp.int32, (chosen, span, rows), 1)
    mask = rank[:, None, :] == slot
    shape = (chosen * span, rows)
    table = mask.astype(f32).reshape(shape).astype(bf16)
    high_ref[...], low_ref[...] = split(jnp.where(mask, weight[:, None, :], 0.0).reshape(shape))
    sent = mm(table, mid).astype(bf16)
    for t, ref in enumerate(sent_refs):
        ref[...] = sent[t * span : (t + 1) * span]


def pack_kernel(*refs):
    refs[-1][...] = jnp.concatenate([ref[...] for ref in refs[:-1]], axis=0)


def expert_kernel(
    own_ref, other_ref, gain_ref, gate_ref, up_ref, down_ref, keep_ref, send_ref, active_ref
):
    tp = lax.axis_index("tp")
    half = own_ref.shape[1]
    low, high = normed(own_ref[...], other_ref[...], gain_ref[...], tp == 0)
    rows = jnp.concatenate([low, high], axis=1)
    hidden = gate_ref.shape[1]
    tile = min(hidden, 256)
    for j in range(hidden // tile):
        part = slice(j * tile, (j + 1) * tile)
        gated = jnp.minimum(mm(rows, gate_ref[:, part]), clamp_limit)
        lifted = jnp.clip(mm(rows, up_ref[:, part]), -clamp_limit, clamp_limit) + 1.0
        active_ref[:, part] = (lifted * gated * jax.nn.sigmoid(swish_alpha * gated)).astype(bf16)
    active = active_ref[...]
    tile = min(half, 256)
    for ref, start in ((send_ref, (1 - tp) * half), (keep_ref, tp * half)):
        for j in range(half // tile):
            part = pl.ds(pl.multiple_of(start + j * tile, tile), tile)
            ref[:, j * tile : (j + 1) * tile] = mm(active, down_ref[:, part]).astype(bf16)


def add_kernel(keep_ref, other_ref, *out_refs):
    span = out_refs[0].shape[0]
    total = (keep_ref[...].astype(f32) + other_ref[...].astype(f32)).astype(bf16)
    for t, ref in enumerate(out_refs):
        ref[...] = total[t * span : (t + 1) * span]


def combine_kernel(high_ref, low_ref, mid_ref, *refs):
    sum_ref, far_ref = refs[-2:]
    back = jnp.concatenate([ref[...] for ref in refs[:-2]], axis=0)
    total = mm(high_ref[...], back, TN) + mm(low_ref[...], back, TN)
    rows = sum_ref.shape[0]
    far_ref[...] = total[rows:].astype(bf16)
    sum_ref[...] = mid_ref[...].astype(f32) + total[:rows]


def final_kernel(sum_ref, far_ref, out_ref):
    out_ref[...] = (sum_ref[...] + far_ref[...].astype(f32)).astype(bf16)


def call(kernel, outs, flops, vmem=8, **more):
    return pl.pallas_call(
        kernel,
        out_shape=tuple(jax.ShapeDtypeStruct(shape, dtype) for shape, dtype in outs),
        compiler_params=pltpu.CompilerParams(vmem_limit_bytes=vmem * 1024 * 1024),
        cost_estimate=pl.CostEstimate(flops=flops, bytes_accessed=10**6, transcendentals=0),
        **more,
    )


def local(
    residual,
    route_ids,
    route_weights,
    carried_state,
    mix_gain,
    in_proj,
    decay_rate,
    frequency,
    step_size,
    input_map,
    output_matrix,
    passthrough_scale,
    out_gain,
    out_proj,
    ffn_gain,
    w_gate,
    w_up,
    w_down,
):
    rows, half = residual.shape
    top = route_ids.shape[1]
    peers = lax.axis_size("ep")
    experts = w_gate.shape[0] * peers
    capacity = max(2, 3 * rows * top // (2 * experts))
    inner = peers // 2
    span = -(-2 * capacity // 16) * 16
    slots = inner * span
    channel_half = in_proj.shape[1]
    hidden = w_gate.shape[2]
    gate, up, down = w_gate[0], w_up[0], w_down[0]

    def across(values):
        return lax.ppermute(values, "tp", [(0, 1), (1, 0)])

    def opposite(values):
        return lax.ppermute(values, "ep", [(e, e ^ inner) for e in range(peers)])

    def within(values, t):
        return lax.ppermute(values, "ep", [(e, e ^ t) for e in range(peers)])

    other = across(residual)
    far_residual = opposite(residual)
    (head,) = call(head_kernel, [((8, 128), f32)], HEAD_FLOPS)()
    operands = (
        decay_rate,
        frequency,
        step_size.reshape(1, -1),
        jnp.swapaxes(input_map, 2, 3),
        output_matrix,
        residual,
        other,
        mix_gain.reshape(1, -1),
        in_proj,
        passthrough_scale.reshape(1, -1),
        route_ids.T,
        route_weights.T,
        carried_state,
        head,
    )
    active, new_state = call(
        mixer_kernel,
        [((rows + 8, channel_half), bf16), (carried_state.shape, f32)],
        10**9,
        MIXER_VMEM,
    )(*operands)
    far_active = opposite(active)
    mid, high, low, *sent = call(
        functools.partial(dispatch_kernel, inner, span, top),
        [((rows, half), bf16)]
        + [((slots, 2 * rows), bf16)] * 2
        + [((span, half), bf16)] * inner,
        10**10,
    )(
        active,
        across(active),
        far_active,
        across(far_active),
        out_gain.reshape(1, -1),
        out_proj,
        residual,
        far_residual,
    )
    got = {t: within(sent[t], t) for t in range(1, inner)}
    got[0] = sent[0]
    back = []
    for turns in (range(inner // 2), range(inner // 2, inner)):
        share = len(turns) * span
        (packed,) = call(pack_kernel, [((share, half), bf16)], 10**6)(*[got[t] for t in turns])
        keep, send = call(
            expert_kernel,
            [((share, half), bf16)] * 2,
            12 * share * half * hidden,
            scratch_shapes=[pltpu.VMEM((share, hidden), bf16)],
        )(packed, across(packed), ffn_gain.reshape(1, -1), gate, up, down)
        sums = call(add_kernel, [((span, half), bf16)] * len(turns), 10**6)(keep, across(send))
        back += [within(value, t) if t else value for t, value in zip(turns, sums)]
    total, far = call(
        combine_kernel, [((rows, half), f32), ((rows, half), bf16)], 10**8
    )(high, low, mid, *back)
    (updated,) = call(final_kernel, [((rows, half), bf16)], 10**6)(total, opposite(far))
    return updated, new_state


def solution(mesh):
    placed = (
        P("ep", "tp"),
        P("ep", None),
        P("ep", None),
        P(None, "ep", "tp"),
        P(),
        P(None, "tp"),
        P("tp", None),
        P("tp", None),
        P("tp"),
        P(None, "tp", None, None),
        P(None, "tp", None, None),
        P("tp"),
        P(),
        P(None, "tp"),
        P(),
        P("ep", None, "tp"),
        P("ep", None, "tp"),
        P("ep", "tp", None),
    )

    return jax.shard_map(
        local,
        mesh=mesh,
        in_specs=placed,
        out_specs=(P("ep", "tp"), P(None, "ep", "tp")),
        check_vma=False,
    )
```

profile of v0, /device:TPU:0, one launch (start us, length us, event | category | flops | bytes accessed | tf_op | source)
XLA Modules:
  0.0 74.2 jit_solution(7528455078259953135)
XLA Ops:
  0.6 0.0 copy-start.7
  0.8 0.6 collective-permute-start
  1.3 1.2 %collective-permute-done.refs_6_ = bf16[64,1024]{1,0:T(8,128)(2,1)S(1)} collective-permute-done((bf16[64,1024]{1,0:T(8,128)(2,1)}, bf16[64,1024]{1,0:T(8,128)(2,1)S(1)}, u32[]{:S(2)}, u32[]{:S(2)}) %collective-permute-start) | collective-permute-done | bytes 131104 | tf_op jit(solution)/shard_map/ppermute | solution.py:296
  2.5 0.0 copy-done.6
  2.6 0.1 copy-done.3
  2.7 0.3 copy-done.4
  3.0 2.6 %shard_map.186 = (bf16[72,512]{1,0:T(8,128)(2,1)S(1)}, f32[2,64,2048]{2,1,0:T(8,128)}) custom-call(f32[32,64]{1,0:T(8,128)S(1)} %copy-done.9, f32[32,64]{1,0:T(8,128)S(1)} %copy-done.10, f32[1,32]{1,0:T(1,128)S(1)} %bitcast.24, f32[2,32,16,64]{3,2,1,0:T(8,128)S(1)} %bitcast.17, f32[2,32,16,64]{3,2,1,0:T(8,128)S(1)} %copy-done.6, ...), custom_call_target="tpu_custom_call" | custom-call | flops 1000000000 | bytes 1000000 | tf_op jit(solution)/shard_map/pallas_call | solution.py:323
  5.6 4.1 %collective-permute-start.2 = (bf16[72,512]{1,0:T(8,128)(2,1)S(1)}, bf16[72,512]{1,0:T(8,128)(2,1)S(1)}, u32[]{:S(2)}, u32[]{:S(2)}) collective-permute-start(bf16[72,512]{1,0:T(8,128)(2,1)S(1)} %get-tuple-element.29.own_ref), channel_id=1, source_target_pairs={{0,16},{2,18},{4,20},{6,22},{8,24},{10,26},{12,28},{14,30},{16,0},... | collective-permute-start | bytes 221192 | tf_op jit(solution)/shard_map/ppermute | solution.py:299
  9.7 0.0 collective-permute-start.4
  9.7 0.0 collective-permute-start.1
  9.7 6.9 %collective-permute-done.2.far_own_ref = bf16[72,512]{1,0:T(8,128)(2,1)S(1)} collective-permute-done((bf16[72,512]{1,0:T(8,128)(2,1)S(1)}, bf16[72,512]{1,0:T(8,128)(2,1)S(1)}, u32[]{:S(2)}, u32[]{:S(2)}) %collective-permute-start.2) | collective-permute-done | bytes 73760 | tf_op jit(solution)/shard_map/ppermute | solution.py:299
  16.6 0.0 collective-permute-start.3
  16.6 2.6 %collective-permute-done.4.far_residual_ref = bf16[64,1024]{1,0:T(8,128)(2,1)S(1)} collective-permute-done((bf16[64,1024]{1,0:T(8,128)(2,1)S(1)}, bf16[64,1024]{1,0:T(8,128)(2,1)S(1)}, u32[]{:S(2)}, u32[]{:S(2)}) %collective-permute-start.4) | collective-permute-done | bytes 131104 | tf_op jit(solution)/shard_map/ppermute | solution.py:299
  19.2 0.0 collective-permute-done.1.other_ref
  19.2 0.0 collective-permute-done.3.far_other_ref
  19.2 0.0 copy-start
  19.2 0.0 copy-start.1
  19.2 0.0 copy-start.2
  19.2 0.0 copy-start.8
  19.3 0.9 %shard_map.187 = (bf16[64,1024]{1,0:T(8,128)(2,1)S(1)}, bf16[384,128]{1,0:T(8,128)(2,1)S(1)}, bf16[384,128]{1,0:T(8,128)(2,1)S(1)}, bf16[48,1024]{1,0:T(8,128)(2...) custom-call(bf16[72,512]{1,0:T(8,128)(2,1)S(1)} %get-tuple-element.2, ...), custom_call_target="tpu_custom_call" | custom-call | flops 10000000000 | bytes 1000000 | tf_op jit(solution)/shard_map/pallas_call | solution.py:330
  20.2 0.7 collective-permute-start.13
  20.9 2.5 %collective-permute-start.14 = (bf16[48,1024]{1,0:T(8,128)(2,1)S(1)}, bf16[48,1024]{1,0:T(8,128)(2,1)S(1)}, u32[]{:S(2)}, u32[]{:S(2)}) collective-permute-start(bf16[48,1024]{1,0:T(8,128)(2,1)S(1)} %get-tuple-element.44), channel_id=1, source_target_pairs={{0,10},{2,8},{4,14},{6,12},{8,2},{10,0},{12,6},{14,4},{16,26},{18,... | collective-permute-start | bytes 294920 | tf_op jit(solution)/shard_map/ppermute | solution.py:302
  23.4 1.4 %collective-permute-start.15 = (bf16[48,1024]{1,0:T(8,128)(2,1)S(1)}, bf16[48,1024]{1,0:T(8,128)(2,1)S(1)}, u32[]{:S(2)}, u32[]{:S(2)}) collective-permute-start(bf16[48,1024]{1,0:T(8,128)(2,1)S(1)} %get-tuple-element.45), channel_id=1, source_target_pairs={{0,12},{2,14},{4,8},{6,10},{8,4},{10,6},{12,0},{14,2},{16,28},{18,... | collective-permute-start | bytes 294920 | tf_op jit(solution)/shard_map/ppermute | solution.py:302
  24.8 1.3 %collective-permute-start.16 = (bf16[48,1024]{1,0:T(8,128)(2,1)S(1)}, bf16[48,1024]{1,0:T(8,128)(2,1)S(1)}, u32[]{:S(2)}, u32[]{:S(2)}) collective-permute-start(bf16[48,1024]{1,0:T(8,128)(2,1)S(1)} %get-tuple-element.46), channel_id=1, source_target_pairs={{0,14},{2,12},{4,10},{6,8},{8,6},{10,4},{12,2},{14,0},{16,30},{18,... | collective-permute-start | bytes 294920 | tf_op jit(solution)/shard_map/ppermute | solution.py:302
  26.1 0.0 collective-permute-done.13.refs_0_
  26.1 3.1 %collective-permute-done.14.refs_1_ = bf16[48,1024]{1,0:T(8,128)(2,1)S(1)} collective-permute-done((bf16[48,1024]{1,0:T(8,128)(2,1)S(1)}, bf16[48,1024]{1,0:T(8,128)(2,1)S(1)}, u32[]{:S(2)}, u32[]{:S(2)}) %collective-permute-start.14) | collective-permute-done | bytes 98336 | tf_op jit(solution)/shard_map/ppermute | solution.py:302
  29.1 2.0 %collective-permute-done.15.refs_2_ = bf16[48,1024]{1,0:T(8,128)(2,1)S(1)} collective-permute-done((bf16[48,1024]{1,0:T(8,128)(2,1)S(1)}, bf16[48,1024]{1,0:T(8,128)(2,1)S(1)}, u32[]{:S(2)}, u32[]{:S(2)}) %collective-permute-start.15) | collective-permute-done | bytes 98336 | tf_op jit(solution)/shard_map/ppermute | solution.py:302
  31.1 1.9 %collective-permute-done.16.refs_3_ = bf16[48,1024]{1,0:T(8,128)(2,1)S(1)} collective-permute-done((bf16[48,1024]{1,0:T(8,128)(2,1)S(1)}, bf16[48,1024]{1,0:T(8,128)(2,1)S(1)}, u32[]{:S(2)}, u32[]{:S(2)}) %collective-permute-start.16) | collective-permute-done | bytes 98336 | tf_op jit(solution)/shard_map/ppermute | solution.py:302
  33.1 0.1 collective-permute-start.17
  33.1 0.9 %collective-permute-start.5 = (bf16[48,1024]{1,0:T(8,128)(2,1)S(1)}, bf16[48,1024]{1,0:T(8,128)(2,1)S(1)}, u32[]{:S(2)}, u32[]{:S(2)}) collective-permute-start(bf16[48,1024]{1,0:T(8,128)(2,1)S(1)} %get-tuple-element.34), channel_id=1, source_target_pairs={{0,2},{2,0},{4,6},{6,4},{8,10},{10,8},{12,14},{14,12},{16,18},{18,... | collective-permute-start | bytes 294920 | tf_op jit(solution)/shard_map/ppermute | solution.py:302
  34.1 0.4 collective-permute-start.6
  34.4 2.2 %collective-permute-start.7 = (bf16[48,1024]{1,0:T(8,128)(2,1)S(1)}, bf16[48,1024]{1,0:T(8,128)(2,1)S(1)}, u32[]{:S(2)}, u32[]{:S(2)}) collective-permute-start(bf16[48,1024]{1,0:T(8,128)(2,1)S(1)} %get-tuple-element.36), channel_id=1, source_target_pairs={{0,6},{2,4},{4,2},{6,0},{8,14},{10,12},{12,10},{14,8},{16,22},{18,... | collective-permute-start | bytes 294920 | tf_op jit(solution)/shard_map/ppermute | solution.py:302
  36.7 2.0 %collective-permute-done.5.refs_1_ = bf16[48,1024]{1,0:T(8,128)(2,1)S(1)} collective-permute-done((bf16[48,1024]{1,0:T(8,128)(2,1)S(1)}, bf16[48,1024]{1,0:T(8,128)(2,1)S(1)}, u32[]{:S(2)}, u32[]{:S(2)}) %collective-permute-start.5) | collective-permute-done | bytes 98336 | tf_op jit(solution)/shard_map/ppermute | solution.py:302
  38.7 2.4 %collective-permute-done.6.refs_2_ = bf16[48,1024]{1,0:T(8,128)(2,1)S(1)} collective-permute-done((bf16[48,1024]{1,0:T(8,128)(2,1)S(1)}, bf16[48,1024]{1,0:T(8,128)(2,1)S(1)}, u32[]{:S(2)}, u32[]{:S(2)}) %collective-permute-start.6) | collective-permute-done | bytes 98336 | tf_op jit(solution)/shard_map/ppermute | solution.py:302
  41.0 0.0 collective-permute-done.7.refs_3_
  41.1 0.1 collective-permute-start.8
  41.1 0.0 collective-permute-done.17.other_ref
  41.2 3.0 %shard_map.192 = (bf16[192,1024]{1,0:T(8,128)(2,1)S(1)}, bf16[192,1024]{1,0:T(8,128)(2,1)S(1)}) custom-call(bf16[192,1024]{1,0:T(8,128)(2,1)S(1)} %shard_map.191.own_ref, bf16[192,1024]{1,0:T(8,128)(2,1)S(1)} %collective-permute-done.17.other_ref, f32[1,2048]{1,0:T(1,128)S(1)} %bitcast.18, bf16[2048,1024]{1,0:T(8,128)(2,1)S(1)} %bitcast.11, ...), custom_call_target="tpu_custom_call" | custom-call | flops 2415919104 | bytes 1000000 | tf_op jit(solution)/shard_map/pallas_call | solution.py:352
  44.2 0.5 collective-permute-start.18
  44.8 0.0 collective-permute-done.8.other_ref
  44.8 3.0 %shard_map.189 = (bf16[192,1024]{1,0:T(8,128)(2,1)S(1)}, bf16[192,1024]{1,0:T(8,128)(2,1)S(1)}) custom-call(bf16[192,1024]{1,0:T(8,128)(2,1)S(1)} %shard_map.188.own_ref, bf16[192,1024]{1,0:T(8,128)(2,1)S(1)} %collective-permute-done.8.other_ref, f32[1,2048]{1,0:T(1,128)S(1)} %bitcast.19, bf16[2048,1024]{1,0:T(8,128)(2,1)S(1)} %bitcast.12, ...), custom_call_target="tpu_custom_call" | custom-call | flops 2415919104 | bytes 1000000 | tf_op jit(solution)/shard_map/pallas_call | solution.py:352
  47.8 0.1 collective-permute-start.9
  47.9 0.0 collective-permute-done.18.other_ref
  47.9 0.1 shard_map.193
  48.0 0.5 collective-permute-start.19
  48.6 2.1 %collective-permute-start.20 = (bf16[48,1024]{1,0:T(8,128)(2,1)S(1)}, bf16[48,1024]{1,0:T(8,128)(2,1)S(1)}, u32[]{:S(2)}, u32[]{:S(2)}) collective-permute-start(bf16[48,1024]{1,0:T(8,128)(2,1)S(1)} %get-tuple-element.50), channel_id=1, source_target_pairs={{0,10},{2,8},{4,14},{6,12},{8,2},{10,0},{12,6},{14,4},{16,26},{18,... | collective-permute-start | bytes 294920 | tf_op jit(solution)/shard_map/ppermute | solution.py:302
  50.7 0.8 %collective-permute-start.21 = (bf16[48,1024]{1,0:T(8,128)(2,1)S(1)}, bf16[48,1024]{1,0:T(8,128)(2,1)S(1)}, u32[]{:S(2)}, u32[]{:S(2)}) collective-permute-start(bf16[48,1024]{1,0:T(8,128)(2,1)S(1)} %get-tuple-element.51), channel_id=1, source_target_pairs={{0,12},{2,14},{4,8},{6,10},{8,4},{10,6},{12,0},{14,2},{16,28},{18,... | collective-permute-start | bytes 294920 | tf_op jit(solution)/shard_map/ppermute | solution.py:302
  51.5 2.4 %collective-permute-start.22 = (bf16[48,1024]{1,0:T(8,128)(2,1)S(1)}, bf16[48,1024]{1,0:T(8,128)(2,1)S(1)}, u32[]{:S(2)}, u32[]{:S(2)}) collective-permute-start(bf16[48,1024]{1,0:T(8,128)(2,1)S(1)} %get-tuple-element.52), channel_id=1, source_target_pairs={{0,14},{2,12},{4,10},{6,8},{8,6},{10,4},{12,2},{14,0},{16,30},{18,... | collective-permute-start | bytes 294920 | tf_op jit(solution)/shard_map/ppermute | solution.py:302
  53.9 0.0 collective-permute-done.9.other_ref
  53.9 0.1 shard_map.190
  54.0 1.2 %collective-permute-start.10 = (bf16[48,1024]{1,0:T(8,128)(2,1)S(1)}, bf16[48,1024]{1,0:T(8,128)(2,1)S(1)}, u32[]{:S(2)}, u32[]{:S(2)}) collective-permute-start(bf16[48,1024]{1,0:T(8,128)(2,1)S(1)} %get-tuple-element.40), channel_id=1, source_target_pairs={{0,2},{2,0},{4,6},{6,4},{8,10},{10,8},{12,14},{14,12},{16,18},{18,... | collective-permute-start | bytes 294920 | tf_op jit(solution)/shard_map/ppermute | solution.py:302
  55.3 0.0 collective-permute-done.19.refs_4_
  55.3 0.6 collective-permute-start.11
  55.9 0.6 collective-permute-done.20.refs_5_
  56.5 1.2 %collective-permute-start.12 = (bf16[48,1024]{1,0:T(8,128)(2,1)S(1)}, bf16[48,1024]{1,0:T(8,128)(2,1)S(1)}, u32[]{:S(2)}, u32[]{:S(2)}) collective-permute-start(bf16[48,1024]{1,0:T(8,128)(2,1)S(1)} %get-tuple-element.42), channel_id=1, source_target_pairs={{0,6},{2,4},{4,2},{6,0},{8,14},{10,12},{12,10},{14,8},{16,22},{18,... | collective-permute-start | bytes 294920 | tf_op jit(solution)/shard_map/ppermute | solution.py:302
  57.6 0.6 collective-permute-done.21.refs_6_
  58.3 2.0 %collective-permute-done.22.refs_7_ = bf16[48,1024]{1,0:T(8,128)(2,1)S(1)} collective-permute-done((bf16[48,1024]{1,0:T(8,128)(2,1)S(1)}, bf16[48,1024]{1,0:T(8,128)(2,1)S(1)}, u32[]{:S(2)}, u32[]{:S(2)}) %collective-permute-start.22) | collective-permute-done | bytes 98336 | tf_op jit(solution)/shard_map/ppermute | solution.py:302
  60.3 1.3 %collective-permute-done.10.refs_1_ = bf16[48,1024]{1,0:T(8,128)(2,1)S(1)} collective-permute-done((bf16[48,1024]{1,0:T(8,128)(2,1)S(1)}, bf16[48,1024]{1,0:T(8,128)(2,1)S(1)}, u32[]{:S(2)}, u32[]{:S(2)}) %collective-permute-start.10) | collective-permute-done | bytes 98336 | tf_op jit(solution)/shard_map/ppermute | solution.py:302
  61.6 2.5 %collective-permute-done.11.refs_2_ = bf16[48,1024]{1,0:T(8,128)(2,1)S(1)} collective-permute-done((bf16[48,1024]{1,0:T(8,128)(2,1)S(1)}, bf16[48,1024]{1,0:T(8,128)(2,1)S(1)}, u32[]{:S(2)}, u32[]{:S(2)}) %collective-permute-start.11) | collective-permute-done | bytes 98336 | tf_op jit(solution)/shard_map/ppermute | solution.py:302
  64.1 0.0 collective-permute-done.12.refs_3_
  64.1 0.5 shard_map.194
  64.6 2.5 %collective-permute-start.23 = (bf16[64,1024]{1,0:T(8,128)(2,1)S(1)}, bf16[64,1024]{1,0:T(8,128)(2,1)S(1)}, u32[]{:S(2)}, u32[]{:S(2)}) collective-permute-start(bf16[64,1024]{1,0:T(8,128)(2,1)S(1)} %get-tuple-element.54), channel_id=1, source_target_pairs={{0,16},{2,18},{4,20},{6,22},{8,24},{10,26},{12,28},{14,30},{16,0},... | collective-permute-start | bytes 393224 | tf_op jit(solution)/shard_map/ppermute | solution.py:299
  67.1 6.4 %collective-permute-done.23.far_ref = bf16[64,1024]{1,0:T(8,128)(2,1)S(1)} collective-permute-done((bf16[64,1024]{1,0:T(8,128)(2,1)S(1)}, bf16[64,1024]{1,0:T(8,128)(2,1)S(1)}, u32[]{:S(2)}, u32[]{:S(2)}) %collective-permute-start.23) | collective-permute-done | bytes 131104 | tf_op jit(solution)/shard_map/ppermute | solution.py:299
  73.5 0.7 shard_map.195
  (31 shorter events, 0.1 us)
Async XLA Ops:
  0.6 1.9 %copy-start.7 = (bf16[64,1024]{1,0:T(8,128)(2,1)S(1)}, bf16[64,1024]{1,0:T(8,128)(2,1)}, u32[]{:S(2)}) copy-start(bf16[64,1024]{1,0:T(8,128)(2,1)} %residual_ref.1) | copy-start | bytes 393220
  0.6 1.9 %copy-start.12 = (f32[512]{0:T(512)S(1)}, f32[512]{0:T(512)}, u32[]{:S(2)}) copy-start(f32[512]{0:T(512)} %param.29) | copy-start | bytes 6148
  0.7 1.9 %copy-start.6 = (f32[2,32,16,64]{3,2,1,0:T(8,128)S(1)}, f32[2,32,16,64]{3,2,1,0:T(8,128)}, u32[]{:S(2)}) copy-start(f32[2,32,16,64]{3,2,1,0:T(8,128)} %refs_4_.1) | copy-start | bytes 786436
  0.7 1.9 %copy-start.5 = (f32[2,32,64,16]{2,3,1,0:T(8,128)S(1)}, f32[2,32,64,16]{2,3,1,0:T(8,128)}, u32[]{:S(2)}) copy-start(f32[2,32,64,16]{2,3,1,0:T(8,128)} %param.27) | copy-start | bytes 786436
  0.7 1.9 %copy-start.15 = (f32[32]{0:T(128)S(1)}, f32[32]{0:T(128)}, u32[]{:S(2)}) copy-start(f32[32]{0:T(128)} %param.26) | copy-start | bytes 388
  0.7 1.9 %copy-start.10 = (f32[32,64]{1,0:T(8,128)S(1)}, f32[32,64]{1,0:T(8,128)}, u32[]{:S(2)}) copy-start(f32[32,64]{1,0:T(8,128)} %refs_1_.1) | copy-start | bytes 24580
  0.7 1.9 %copy-start.9 = (f32[32,64]{1,0:T(8,128)S(1)}, f32[32,64]{1,0:T(8,128)}, u32[]{:S(2)}) copy-start(f32[32,64]{1,0:T(8,128)} %refs_0_.1) | copy-start | bytes 24580
  0.7 2.0 %copy-start.3 = (bf16[2048,512]{1,0:T(8,128)(2,1)S(1)}, bf16[2048,512]{1,0:T(8,128)(2,1)}, u32[]{:S(2)}) copy-start(bf16[2048,512]{1,0:T(8,128)(2,1)} %refs_8_.1) | copy-start | bytes 6291460
  0.7 2.0 %copy-start.11 = (f32[2048]{0:T(1024)S(1)}, f32[2048]{0:T(1024)}, u32[]{:S(2)}) copy-start(f32[2048]{0:T(1024)} %param.22) | copy-start | bytes 24580
  0.7 2.2 %copy-start.4 = (f32[2,64,2048]{2,1,0:T(8,128)S(1)}, f32[2,64,2048]{2,1,0:T(8,128)}, u32[]{:S(2)}) copy-start(f32[2,64,2048]{2,1,0:T(8,128)} %refs_12_.1) | copy-start | bytes 3145732
  0.7 2.2 %copy-start.14 = (f32[64,4]{0,1:T(4,128)S(1)}, f32[64,4]{0,1:T(4,128)}, u32[]{:S(2)}) copy-start(f32[64,4]{0,1:T(4,128)} %param.20) | copy-start | bytes 3076
  0.7 2.2 %copy-start.13 = (s32[64,4]{0,1:T(4,128)S(1)}, s32[64,4]{0,1:T(4,128)}, u32[]{:S(2)}) copy-start(s32[64,4]{0,1:T(4,128)} %param.19) | copy-start | bytes 3076
  0.8 1.8 %collective-permute-start = (bf16[64,1024]{1,0:T(8,128)(2,1)}, bf16[64,1024]{1,0:T(8,128)(2,1)S(1)}, u32[]{:S(2)}, u32[]{:S(2)}) collective-permute-start(bf16[64,1024]{1,0:T(8,128)(2,1)} %residual_ref.1), channel_id=1, source_target_pairs={{0,1},{1,0},{2,3},{3,2},{4,5},{5,4},{6,7},{7,6},{8,9},{9,8},{10,11... | collective-permute-start | bytes 393224 | tf_op jit(solution)/shard_map/ppermute | solution.py:296
  1.3 17.9 %copy-start.16 = (bf16[1024,1024]{1,0:T(8,128)(2,1)S(1)}, bf16[1024,1024]{1,0:T(8,128)(2,1)}, u32[]{:S(2)}) copy-start(bf16[1024,1024]{1,0:T(8,128)(2,1)} %proj_ref.1) | copy-start | bytes 6291460
  1.3 17.9 %copy-start.17 = (f32[1024]{0:T(1024)S(1)}, f32[1024]{0:T(1024)}, u32[]{:S(2)}) copy-start(f32[1024]{0:T(1024)} %param.30) | copy-start | bytes 12292
  5.6 11.0 %collective-permute-start.2 = (bf16[72,512]{1,0:T(8,128)(2,1)S(1)}, bf16[72,512]{1,0:T(8,128)(2,1)S(1)}, u32[]{:S(2)}, u32[]{:S(2)}) collective-permute-start(bf16[72,512]{1,0:T(8,128)(2,1)S(1)} %get-tuple-element.29.own_ref), channel_id=1, source_target_pairs={{0,16},{2,18},{4,20},{6,22},{8,24},{10,26},{12,28},{14,30},{16,0},... | collective-permute-start | bytes 221192 | tf_op jit(solution)/shard_map/ppermute | solution.py:299
  9.7 9.5 %collective-permute-start.4 = (bf16[64,1024]{1,0:T(8,128)(2,1)S(1)}, bf16[64,1024]{1,0:T(8,128)(2,1)S(1)}, u32[]{:S(2)}, u32[]{:S(2)}) collective-permute-start(bf16[64,1024]{1,0:T(8,128)(2,1)S(1)} %copy-done.7), channel_id=1, source_target_pairs={{0,16},{2,18},{4,20},{6,22},{8,24},{10,26},{12,28},{14,30},{16,0},... | collective-permute-start | bytes 393224 | tf_op jit(solution)/shard_map/ppermute | solution.py:299
  9.7 9.5 %collective-permute-start.1 = (bf16[72,512]{1,0:T(8,128)(2,1)S(1)}, bf16[72,512]{1,0:T(8,128)(2,1)S(1)}, u32[]{:S(2)}, u32[]{:S(2)}) collective-permute-start(bf16[72,512]{1,0:T(8,128)(2,1)S(1)} %get-tuple-element.29.own_ref), channel_id=1, source_target_pairs={{0,1},{1,0},{2,3},{3,2},{4,5},{5,4},{6,7},{7,6},{8,9},{9,8},{10,11... | collective-permute-start | bytes 221192 | tf_op jit(solution)/shard_map/ppermute | solution.py:296
  16.6 2.6 %collective-permute-start.3 = (bf16[72,512]{1,0:T(8,128)(2,1)S(1)}, bf16[72,512]{1,0:T(8,128)(2,1)S(1)}, u32[]{:S(2)}, u32[]{:S(2)}) collective-permute-start(bf16[72,512]{1,0:T(8,128)(2,1)S(1)} %collective-permute-done.2.far_own_ref), channel_id=1, source_target_pairs={{0,1},{1,0},{2,3},{3,2},{4,5},{5,4},{6,7},{7,6},{8,9},{9,8},{10,11... | collective-permute-start | bytes 221192 | tf_op jit(solution)/shard_map/ppermute | solution.py:296
  19.2 21.9 %copy-start = (bf16[1,2048,1024]{2,1,0:T(8,128)(2,1)S(1)}, bf16[1,2048,1024]{2,1,0:T(8,128)(2,1)}, u32[]{:S(2)}) copy-start(bf16[1,2048,1024]{2,1,0:T(8,128)(2,1)} %param.33) | copy-start | bytes 12582916
  19.2 21.9 %copy-start.1 = (bf16[1,2048,1024]{2,1,0:T(8,128)(2,1)S(1)}, bf16[1,2048,1024]{2,1,0:T(8,128)(2,1)}, u32[]{:S(2)}) copy-start(bf16[1,2048,1024]{2,1,0:T(8,128)(2,1)} %param.34) | copy-start | bytes 12582916
  19.2 21.9 %copy-start.2 = (bf16[1,1024,2048]{2,1,0:T(8,128)(2,1)S(1)}, bf16[1,1024,2048]{2,1,0:T(8,128)(2,1)}, u32[]{:S(2)}) copy-start(bf16[1,1024,2048]{2,1,0:T(8,128)(2,1)} %param.35) | copy-start | bytes 12582916
  19.2 21.9 %copy-start.8 = (f32[2048]{0:T(1024)S(1)}, f32[2048]{0:T(1024)}, u32[]{:S(2)}) copy-start(f32[2048]{0:T(1024)} %param.32) | copy-start | bytes 24580
  20.2 5.9 %collective-permute-start.13 = (bf16[48,1024]{1,0:T(8,128)(2,1)S(1)}, bf16[48,1024]{1,0:T(8,128)(2,1)S(1)}, u32[]{:S(2)}, u32[]{:S(2)}) collective-permute-start(bf16[48,1024]{1,0:T(8,128)(2,1)S(1)} %get-tuple-element.43), channel_id=1, source_target_pairs={{0,8},{2,10},{4,12},{6,14},{8,0},{10,2},{12,4},{14,6},{16,24},{18,... | collective-permute-start | bytes 294920 | tf_op jit(solution)/shard_map/ppermute | solution.py:302
  20.9 8.2 %collective-permute-start.14 = (bf16[48,1024]{1,0:T(8,128)(2,1)S(1)}, bf16[48,1024]{1,0:T(8,128)(2,1)S(1)}, u32[]{:S(2)}, u32[]{:S(2)}) collective-permute-start(bf16[48,1024]{1,0:T(8,128)(2,1)S(1)} %get-tuple-element.44), channel_id=1, source_target_pairs={{0,10},{2,8},{4,14},{6,12},{8,2},{10,0},{12,6},{14,4},{16,26},{18,... | collective-permute-start | bytes 294920 | tf_op jit(solution)/shard_map/ppermute | solution.py:302
  23.4 7.7 %collective-permute-start.15 = (bf16[48,1024]{1,0:T(8,128)(2,1)S(1)}, bf16[48,1024]{1,0:T(8,128)(2,1)S(1)}, u32[]{:S(2)}, u32[]{:S(2)}) collective-permute-start(bf16[48,1024]{1,0:T(8,128)(2,1)S(1)} %get-tuple-element.45), channel_id=1, source_target_pairs={{0,12},{2,14},{4,8},{6,10},{8,4},{10,6},{12,0},{14,2},{16,28},{18,... | collective-permute-start | bytes 294920 | tf_op jit(solution)/shard_map/ppermute | solution.py:302
  24.8 8.2 %collective-permute-start.16 = (bf16[48,1024]{1,0:T(8,128)(2,1)S(1)}, bf16[48,1024]{1,0:T(8,128)(2,1)S(1)}, u32[]{:S(2)}, u32[]{:S(2)}) collective-permute-start(bf16[48,1024]{1,0:T(8,128)(2,1)S(1)} %get-tuple-element.46), channel_id=1, source_target_pairs={{0,14},{2,12},{4,10},{6,8},{8,6},{10,4},{12,2},{14,0},{16,30},{18,... | collective-permute-start | bytes 294920 | tf_op jit(solution)/shard_map/ppermute | solution.py:302
  33.1 8.1 %collective-permute-start.17 = (bf16[192,1024]{1,0:T(8,128)(2,1)S(1)}, bf16[192,1024]{1,0:T(8,128)(2,1)S(1)}, u32[]{:S(2)}, u32[]{:S(2)}) collective-permute-start(bf16[192,1024]{1,0:T(8,128)(2,1)S(1)} %shard_map.191.own_ref), channel_id=1, source_target_pairs={{0,1},{1,0},{2,3},{3,2},{4,5},{5,4},{6,7},{7,6},{8,9},{9,8},{10,11... | collective-permute-start | bytes 1179656 | tf_op jit(solution)/shard_map/ppermute | solution.py:296
  33.1 5.5 %collective-permute-start.5 = (bf16[48,1024]{1,0:T(8,128)(2,1)S(1)}, bf16[48,1024]{1,0:T(8,128)(2,1)S(1)}, u32[]{:S(2)}, u32[]{:S(2)}) collective-permute-start(bf16[48,1024]{1,0:T(8,128)(2,1)S(1)} %get-tuple-element.34), channel_id=1, source_target_pairs={{0,2},{2,0},{4,6},{6,4},{8,10},{10,8},{12,14},{14,12},{16,18},{18,... | collective-permute-start | bytes 294920 | tf_op jit(solution)/shard_map/ppermute | solution.py:302
  34.1 7.0 %collective-permute-start.6 = (bf16[48,1024]{1,0:T(8,128)(2,1)S(1)}, bf16[48,1024]{1,0:T(8,128)(2,1)S(1)}, u32[]{:S(2)}, u32[]{:S(2)}) collective-permute-start(bf16[48,1024]{1,0:T(8,128)(2,1)S(1)} %get-tuple-element.35), channel_id=1, source_target_pairs={{0,4},{2,6},{4,0},{6,2},{8,12},{10,14},{12,8},{14,10},{16,20},{18,... | collective-permute-start | bytes 294920 | tf_op jit(solution)/shard_map/ppermute | solution.py:302
  34.4 6.6 %collective-permute-start.7 = (bf16[48,1024]{1,0:T(8,128)(2,1)S(1)}, bf16[48,1024]{1,0:T(8,128)(2,1)S(1)}, u32[]{:S(2)}, u32[]{:S(2)}) collective-permute-start(bf16[48,1024]{1,0:T(8,128)(2,1)S(1)} %get-tuple-element.36), channel_id=1, source_target_pairs={{0,6},{2,4},{4,2},{6,0},{8,14},{10,12},{12,10},{14,8},{16,22},{18,... | collective-permute-start | bytes 294920 | tf_op jit(solution)/shard_map/ppermute | solution.py:302
  41.1 3.7 %collective-permute-start.8 = (bf16[192,1024]{1,0:T(8,128)(2,1)S(1)}, bf16[192,1024]{1,0:T(8,128)(2,1)S(1)}, u32[]{:S(2)}, u32[]{:S(2)}) collective-permute-start(bf16[192,1024]{1,0:T(8,128)(2,1)S(1)} %shard_map.188.own_ref), channel_id=1, source_target_pairs={{0,1},{1,0},{2,3},{3,2},{4,5},{5,4},{6,7},{7,6},{8,9},{9,8},{10,11... | collective-permute-start | bytes 1179656 | tf_op jit(solution)/shard_map/ppermute | solution.py:296
  44.2 3.7 %collective-permute-start.18 = (bf16[192,1024]{1,0:T(8,128)(2,1)S(1)}, bf16[192,1024]{1,0:T(8,128)(2,1)S(1)}, u32[]{:S(2)}, u32[]{:S(2)}) collective-permute-start(bf16[192,1024]{1,0:T(8,128)(2,1)S(1)} %get-tuple-element.48), channel_id=1, source_target_pairs={{0,1},{1,0},{2,3},{3,2},{4,5},{5,4},{6,7},{7,6},{8,9},{9,8},{10,11... | collective-permute-start | bytes 1179656 | tf_op jit(solution)/shard_map/ppermute | solution.py:296
  47.8 6.1 %collective-permute-start.9 = (bf16[192,1024]{1,0:T(8,128)(2,1)S(1)}, bf16[192,1024]{1,0:T(8,128)(2,1)S(1)}, u32[]{:S(2)}, u32[]{:S(2)}) collective-permute-start(bf16[192,1024]{1,0:T(8,128)(2,1)S(1)} %get-tuple-element.38), channel_id=1, source_target_pairs={{0,1},{1,0},{2,3},{3,2},{4,5},{5,4},{6,7},{7,6},{8,9},{9,8},{10,11... | collective-permute-start | bytes 1179656 | tf_op jit(solution)/shard_map/ppermute | solution.py:296
  48.0 7.2 %collective-permute-start.19 = (bf16[48,1024]{1,0:T(8,128)(2,1)S(1)}, bf16[48,1024]{1,0:T(8,128)(2,1)S(1)}, u32[]{:S(2)}, u32[]{:S(2)}) collective-permute-start(bf16[48,1024]{1,0:T(8,128)(2,1)S(1)} %get-tuple-element.49), channel_id=1, source_target_pairs={{0,8},{2,10},{4,12},{6,14},{8,0},{10,2},{12,4},{14,6},{16,24},{18,... | collective-permute-start | bytes 294920 | tf_op jit(solution)/shard_map/ppermute | solution.py:302
  48.6 7.9 %collective-permute-start.20 = (bf16[48,1024]{1,0:T(8,128)(2,1)S(1)}, bf16[48,1024]{1,0:T(8,128)(2,1)S(1)}, u32[]{:S(2)}, u32[]{:S(2)}) collective-permute-start(bf16[48,1024]{1,0:T(8,128)(2,1)S(1)} %get-tuple-element.50), channel_id=1, source_target_pairs={{0,10},{2,8},{4,14},{6,12},{8,2},{10,0},{12,6},{14,4},{16,26},{18,... | collective-permute-start | bytes 294920 | tf_op jit(solution)/shard_map/ppermute | solution.py:302
  50.7 7.6 %collective-permute-start.21 = (bf16[48,1024]{1,0:T(8,128)(2,1)S(1)}, bf16[48,1024]{1,0:T(8,128)(2,1)S(1)}, u32[]{:S(2)}, u32[]{:S(2)}) collective-permute-start(bf16[48,1024]{1,0:T(8,128)(2,1)S(1)} %get-tuple-element.51), channel_id=1, source_target_pairs={{0,12},{2,14},{4,8},{6,10},{8,4},{10,6},{12,0},{14,2},{16,28},{18,... | collective-permute-start | bytes 294920 | tf_op jit(solution)/shard_map/ppermute | solution.py:302
  51.5 8.8 %collective-permute-start.22 = (bf16[48,1024]{1,0:T(8,128)(2,1)S(1)}, bf16[48,1024]{1,0:T(8,128)(2,1)S(1)}, u32[]{:S(2)}, u32[]{:S(2)}) collective-permute-start(bf16[48,1024]{1,0:T(8,128)(2,1)S(1)} %get-tuple-element.52), channel_id=1, source_target_pairs={{0,14},{2,12},{4,10},{6,8},{8,6},{10,4},{12,2},{14,0},{16,30},{18,... | collective-permute-start | bytes 294920 | tf_op jit(solution)/shard_map/ppermute | solution.py:302
  54.0 7.5 %collective-permute-start.10 = (bf16[48,1024]{1,0:T(8,128)(2,1)S(1)}, bf16[48,1024]{1,0:T(8,128)(2,1)S(1)}, u32[]{:S(2)}, u32[]{:S(2)}) collective-permute-start(bf16[48,1024]{1,0:T(8,128)(2,1)S(1)} %get-tuple-element.40), channel_id=1, source_target_pairs={{0,2},{2,0},{4,6},{6,4},{8,10},{10,8},{12,14},{14,12},{16,18},{18,... | collective-permute-start | bytes 294920 | tf_op jit(solution)/shard_map/ppermute | solution.py:302
  55.3 8.8 %collective-permute-start.11 = (bf16[48,1024]{1,0:T(8,128)(2,1)S(1)}, bf16[48,1024]{1,0:T(8,128)(2,1)S(1)}, u32[]{:S(2)}, u32[]{:S(2)}) collective-permute-start(bf16[48,1024]{1,0:T(8,128)(2,1)S(1)} %get-tuple-element.41), channel_id=1, source_target_pairs={{0,4},{2,6},{4,0},{6,2},{8,12},{10,14},{12,8},{14,10},{16,20},{18,... | collective-permute-start | bytes 294920 | tf_op jit(solution)/shard_map/ppermute | solution.py:302
  56.5 7.7 %collective-permute-start.12 = (bf16[48,1024]{1,0:T(8,128)(2,1)S(1)}, bf16[48,1024]{1,0:T(8,128)(2,1)S(1)}, u32[]{:S(2)}, u32[]{:S(2)}) collective-permute-start(bf16[48,1024]{1,0:T(8,128)(2,1)S(1)} %get-tuple-element.42), channel_id=1, source_target_pairs={{0,6},{2,4},{4,2},{6,0},{8,14},{10,12},{12,10},{14,8},{16,22},{18,... | collective-permute-start | bytes 294920 | tf_op jit(solution)/shard_map/ppermute | solution.py:302
  64.6 8.9 %collective-permute-start.23 = (bf16[64,1024]{1,0:T(8,128)(2,1)S(1)}, bf16[64,1024]{1,0:T(8,128)(2,1)S(1)}, u32[]{:S(2)}, u32[]{:S(2)}) collective-permute-start(bf16[64,1024]{1,0:T(8,128)(2,1)S(1)} %get-tuple-element.54), channel_id=1, source_target_pairs={{0,16},{2,18},{4,20},{6,22},{8,24},{10,26},{12,28},{14,30},{16,0},... | collective-permute-start | bytes 393224 | tf_op jit(solution)/shard_map/ppermute | solution.py:299
where the time goes:
time: 74.3 us; the launch traced here: 74.2 us
  waiting for transfers between devices  35.4 us (48%)
  starting transfers between devices  26.3 us (35%)
  Pallas kernels  11 us (15%)
  between operations  0.93 us (1%)
    ppermute x14, starting transfers between devices, within(): return lax.ppermute(values, 'ep', [(e, e ^ t) for e in range(peers)])  18.4 us
    ppermute x14, waiting for transfers between devices, within(): return lax.ppermute(values, 'ep', [(e, e ^ t) for e in range(peers)])  18.4 us
    ppermute x3, waiting for transfers between devices, opposite(): return lax.ppermute(values, 'ep', [(e, e ^ inner) for e in range(peers)])  15.9 us
    ppermute x3, starting transfers between devices, opposite(): return lax.ppermute(values, 'ep', [(e, e ^ inner) for e in range(peers)])  6.59 us
    pallas_call x2, Pallas kernels, local(): call(expert_kernel, [((share, half), bf16)] * 2, 12 * share * half * hidd...  6.08 us
    pallas_call x1, Pallas kernels, local(): call(mixer_kernel, [((rows + 8, channel_half), bf16), (carried_state.shap...  2.62 us
  transfers between devices with their start and end apart: 24, of which 14 were waited for; matrix products, arithmetic and copies ran while one was open for 0% of the time, Pallas kernels for 8%

commit v1 on v0

--- a/solution.py
+++ b/solution.py
@@ -133,8 +133,46 @@
     )
 
 
+def tables(own_ref, rows, top, chosen, span, turned):
+    half = own_ref.shape[1]
+    each = half // rows
+    tags = own_ref[rows:].astype(f32)
+    tags = jnp.concatenate(
+        [
+            tags[i // each : i // each + 1, i % each * rows : (i % each + 1) * rows]
+            for i in range(4 * top)
+        ],
+        axis=0,
+    )
+    ids = tags[:top].astype(jnp.int32)
+    weights = tags[top : 2 * top] + tags[2 * top : 3 * top] + tags[3 * top :]
+    place = lax.axis_index("ep")
+    base = place // chosen * chosen
+    turn = lax.broadcasted_iota(jnp.int32, (chosen, rows), 0)
+    earlier = lax.broadcasted_iota(jnp.int32, (rows, rows), 0) < lax.broadcasted_iota(
+        jnp.int32, (rows, rows), 1
+    )
+    slot = lax.broadcasted_iota(jnp.int32, (chosen, span, rows), 1)
+
+    def masked(expert):
+        named = jnp.zeros((chosen, rows), f32)
+        weight = jnp.zeros((chosen, rows), f32)
+        for k in range(top):
+            same = ids[k : k + 1, :] == expert
+            named = named + same.astype(f32)
+            weight = weight + jnp.where(same, weights[k : k + 1, :], 0.0)
+        rank = mm(named.astype(bf16), earlier.astype(f32).astype(bf16))
+        rank = jnp.where(named > 0.0, rank, -1.0).astype(jnp.int32)
+        return rank[:, None, :] == slot, weight[:, None, :]
+
+    selected, weight = masked(base + (turn ^ (place - base)))
+    mask = selected
+    if not turned:
+        mask, weight = masked(base + turn)
+    return selected.astype(f32), jnp.where(mask, weight, 0.0).reshape(chosen * span, rows)
+
+
 def dispatch_kernel(
-    chosen,
     span,
     top,
     own_ref,
@@ -148,106 +186,124 @@
     mid_ref,
     high_ref,
     low_ref,
+    far_high_ref,
+    far_low_ref,
     *sent_refs,
 ):
-    first = lax.axis_index("tp") == 0
-    count = residual_ref.shape[0]
-    own = jnp.concatenate([own_ref[:count], far_own_ref[:count]], axis=0)
-    other = jnp.concatenate([other_ref[:count], far_other_ref[:count]], axis=0)
-    low, high = normed(own, other, gain_ref[...], first)
-    half = own.shape[1]
+    rows = residual_ref.shape[0]
+    chosen = len(sent_refs)
+    own = jnp.concatenate([own_ref[:rows], far_own_ref[:rows]], axis=0)
+    other = jnp.concatenate([other_ref[:rows], far_other_ref[:rows]], axis=0)
+    low, high = normed(own, other, gain_ref[...], lax.axis_index("tp") == 0)
+    half = low.shape[1]
     product = mm(low, proj_ref[:half, :]) + mm(high, proj_ref[half:, :])
     residual = jnp.concatenate([residual_ref[...], far_residual_ref[...]], axis=0)
     mid = (residual.astype(f32) + product).astype(bf16)
-    mid_ref[...] = mid[: mid_ref.shape[0]]
-
-    each = half // count
-    tags = [ref[count:].astype(f32) for ref in (own_ref, far_own_ref)]
-    tags = jnp.concatenate(
-        [
-            jnp.concatenate(
-                [
-                    tag[i // each : i // each + 1, i % each * count : (i % each + 1) * count]
-                    for i in range(4 * top)
-                ],
-                axis=0,
-            )
-            for tag in tags
-        ],
-        axis=1,
-    )
-    rows = tags.shape[1]
-    ids = tags[:top].astype(jnp.int32)
-    weights = tags[top : 2 * top] + tags[2 * top : 3 * top] + tags[3 * top :]
-    place = lax.axis_index("ep")
-    base = place // chosen * chosen
-    turn = lax.broadcasted_iota(jnp.int32, (chosen, rows), 0)
-    expert = base + (turn ^ (place - base))
-    named = jnp.zeros((chosen, rows), f32)
-    weight = jnp.zeros((chosen, rows), f32)
-    for k in range(top):
-        same = ids[k : k + 1, :] == expert
-        named = named + same.astype(f32)
-        weight = weight + jnp.where(same, weights[k : k + 1, :], 0.0)
-    earlier = lax.broadcasted_iota(jnp.int32, (rows, rows), 0) < lax.broadcasted_iota(
-        jnp.int32, (rows, rows), 1
-    )
-    rank = mm(named.astype(bf16), earlier.astype(f32).astype(bf16))
-    rank = jnp.where(named > 0.0, rank, -1.0).astype(jnp.int32)
-    slot = lax.broadcasted_iota(jnp.int32, (chosen, span, rows), 1)
-    mask = rank[:, None, :] == slot
-    shape = (chosen * span, rows)
-    table = mask.astype(f32).reshape(shape).astype(bf16)
-    high_ref[...], low_ref[...] = split(jnp.where(mask, weight[:, None, :], 0.0).reshape(shape))
-    sent = mm(table, mid).astype(bf16)
+    mid_ref[...] = mid[:rows]
+    near, near_weights = tables(own_ref, rows, top, chosen, span, True)
+    far, far_weights = tables(far_own_ref, rows, top, chosen, span, False)
+    high_ref[...], low_ref[...] = split(near_weights)
+    far_high_ref[...], far_low_ref[...] = split(far_weights)
+    none = jnp.zeros_like(near)
+    table = jnp.concatenate(
+        [jnp.concatenate([near, none], axis=2), jnp.concatenate([none, far], axis=2)], axis=1
+    )
+    table = table.reshape(2 * chosen * span, 2 * rows).astype(bf16)
+    sent = mm(table, mid)
     for t, ref in enumerate(sent_refs):
-        ref[...] = sent[t * span : (t + 1) * span]
+        ref[...] = sent[2 * t * span : 2 * (t + 1) * span].astype(bf16)
 
 
 def pack_kernel(*refs):
     refs[-1][...] = jnp.concatenate([ref[...] for ref in refs[:-1]], axis=0)
 
 
-def expert_kernel(
-    own_ref, other_ref, gain_ref, gate_ref, up_ref, down_ref, keep_ref, send_ref, active_ref
-):
-    tp = lax.axis_index("tp")
-    half = own_ref.shape[1]
-    low, high = normed(own_ref[...], other_ref[...], gain_ref[...], tp == 0)
-    rows = jnp.concatenate([low, high], axis=1)
+def scaled_half(ref, gain_ref, side):
+    values = ref[...].astype(f32)
+    width = values.shape[1]
+    total = jnp.sum(values * values, axis=1, keepdims=True)
+    part = pl.ds(pl.multiple_of(side * width, width), width)
+    return (values * gain_ref[:, part]).astype(bf16), total, part
+
+
+def own_kernel(own_ref, gain_ref, gate_ref, up_ref, gate_sum_ref, up_sum_ref, total_ref):
+    rows, total, part = scaled_half(own_ref, gain_ref, lax.axis_index("tp"))
+    total_ref[...] = jnp.broadcast_to(total, total_ref.shape)
     hidden = gate_ref.shape[1]
     tile = min(hidden, 256)
     for j in range(hidden // tile):
-        part = slice(j * tile, (j + 1) * tile)
-        gated = jnp.minimum(mm(rows, gate_ref[:, part]), clamp_limit)
-        lifted = jnp.clip(mm(rows, up_ref[:, part]), -clamp_limit, clamp_limit) + 1.0
-        active_ref[:, part] = (lifted * gated * jax.nn.sigmoid(swish_alpha * gated)).astype(bf16)
+        col = slice(j * tile, (j + 1) * tile)
+        gate_sum_ref[:, col] = mm(rows, gate_ref[part, col])
+        up_sum_ref[:, col] = mm(rows, up_ref[part, col])
+
+
+def expert_kernel(
+    other_ref,
+    gate_sum_ref,
+    up_sum_ref,
+    total_ref,
+    gain_ref,
+    gate_ref,
+    up_ref,
+    down_ref,
+    active_ref,
+    send_ref,
+):
+    theirs = 1 - lax.axis_index("tp")
+    rows, total, part = scaled_half(other_ref, gain_ref, theirs)
+    half = rows.shape[1]
+    scale = lax.rsqrt((total + total_ref[:, :1]) / (2 * half) + epsilon)
+    hidden = gate_ref.shape[1]
+    tile = min(hidden, 256)
+    for j in range(hidden // tile):
+        col = slice(j * tile, (j + 1) * tile)
+        gate = (gate_sum_ref[:, col] + mm(rows, gate_ref[part, col])) * scale
+        up = (up_sum_ref[:, col] + mm(rows, up_ref[part, col])) * scale
+        gated = jnp.minimum(gate, clamp_limit)
+        lifted = jnp.clip(up, -clamp_limit, clamp_limit) + 1.0
+        active_ref[:, col] = (lifted * gated * jax.nn.sigmoid(swish_alpha * gated)).astype(bf16)
+    lower(active_ref, down_ref, theirs, send_ref)
+
+
+def lower(active_ref, down_ref, side, out_ref):
     active = active_ref[...]
+    half = out_ref.shape[1]
     tile = min(half, 256)
-    for ref, start in ((send_ref, (1 - tp) * half), (keep_ref, tp * half)):
-        for j in range(half // tile):
-            part = pl.ds(pl.multiple_of(start + j * tile, tile), tile)
-            ref[:, j * tile : (j + 1) * tile] = mm(active, down_ref[:, part]).astype(bf16)
-
-
-def add_kernel(keep_ref, other_ref, *out_refs):
-    span = out_refs[0].shape[0]
-    total = (keep_ref[...].astype(f32) + other_ref[...].astype(f32)).astype(bf16)
-    for t, ref in enumerate(out_refs):
-        ref[...] = total[t * span : (t + 1) * span]
-
-
-def combine_kernel(high_ref, low_ref, mid_ref, *refs):
-    sum_ref, far_ref = refs[-2:]
-    back = jnp.concatenate([ref[...] for ref in refs[:-2]], axis=0)
-    total = mm(high_ref[...], back, TN) + mm(low_ref[...], back, TN)
-    rows = sum_ref.shape[0]
-    far_ref[...] = total[rows:].astype(bf16)
-    sum_ref[...] = mid_ref[...].astype(f32) + total[:rows]
-
-
-def final_kernel(sum_ref, far_ref, out_ref):
-    out_ref[...] = (sum_ref[...] + far_ref[...].astype(f32)).astype(bf16)
+    for j in range(half // tile):
+        part = pl.ds(pl.multiple_of(side * half + j * tile, tile), tile)
+        out_ref[:, j * tile : (j + 1) * tile] = mm(active, down_ref[:, part]).astype(bf16)
+
+
+def keep_kernel(active_ref, down_ref, keep_ref):
+    lower(active_ref, down_ref, lax.axis_index("tp"), keep_ref)
+
+
+def add_kernel(*refs):
+    refs, far_ref, near_refs = refs[:4], refs[4], refs[5:]
+    chosen, span, _ = far_ref.shape
+    place = lax.axis_index("ep") % chosen
+    first = 0
+    for keep_ref, other_ref in zip(refs[::2], refs[1::2]):
+        total = keep_ref[...].astype(f32) + other_ref[...].astype(f32)
+        for i in range(total.shape[0] // (2 * span)):
+            member = (first + i) ^ place
+            near_refs[first + i][...] = total[2 * i * span : (2 * i + 1) * span].astype(bf16)
+            far_ref[member] = total[(2 * i + 1) * span : 2 * (i + 1) * span].astype(bf16)
+        first += total.shape[0] // (2 * span)
+
+
+def weighted(high_ref, low_ref, refs):
+    back = jnp.concatenate([ref[...].astype(f32) for ref in refs], axis=0).astype(bf16)
+    return mm(high_ref[...], back, TN) + mm(low_ref[...], back, TN)
+
+
+def combine_kernel(high_ref, low_ref, back_ref, out_ref):
+    out_ref[...] = weighted(high_ref, low_ref, (back_ref,)).astype(bf16)
+
+
+def final_kernel(high_ref, low_ref, mid_ref, far_ref, *refs):
+    total = mid_ref[...].astype(f32) + far_ref[...].astype(f32)
+    refs[-1][...] = (total + weighted(high_ref, low_ref, refs[:-1])).astype(bf16)
 
 
 def call(kernel, outs, flops, vmem=8, **more):
@@ -286,7 +342,7 @@
     experts = w_gate.shape[0] * peers
     capacity = max(2, 3 * rows * top // (2 * experts))
     inner = peers // 2
-    span = -(-2 * capacity // 16) * 16
+    span = -(-capacity // 8) * 8
     slots = inner * span
     channel_half = in_proj.shape[1]
     hidden = w_gate.shape[2]
@@ -300,6 +356,14 @@
 
     def within(values, t):
         return lax.ppermute(values, "ep", [(e, e ^ t) for e in range(peers)])
+
+    cubes = [[h * inner + i for i in range(inner)] for h in range(2)]
+
+    def returned(values):
+        values = lax.all_to_all(
+            values, "ep", split_axis=0, concat_axis=0, tiled=True, axis_index_groups=cubes
+        )
+        return values.reshape(slots, half)
 
     other = across(residual)
     far_residual = opposite(residual)
@@ -327,11 +391,11 @@
         MIXER_VMEM,
     )(*operands)
     far_active = opposite(active)
-    mid, high, low, *sent = call(
-        functools.partial(dispatch_kernel, inner, span, top),
+    mid, high, low, far_high, far_low, *sent = call(
+        functools.partial(dispatch_kernel, span, top),
         [((rows, half), bf16)]
-        + [((slots, 2 * rows), bf16)] * 2
-        + [((span, half), bf16)] * inner,
+        + [((slots, rows), bf16)] * 4
+        + [((2 * span, half), bf16)] * inner,
         10**10,
     )(
         active,
@@ -345,22 +409,34 @@
     )
     got = {t: within(sent[t], t) for t in range(1, inner)}
     got[0] = sent[0]
-    back = []
+    parts = []
     for turns in (range(inner // 2), range(inner // 2, inner)):
-        share = len(turns) * span
+        share = 2 * len(turns) * span
         (packed,) = call(pack_kernel, [((share, half), bf16)], 10**6)(*[got[t] for t in turns])
-        keep, send = call(
+        gain = ffn_gain.reshape(1, -1)
+        partial = call(
+            own_kernel,
+            [((share, hidden), f32)] * 2 + [((share, 128), f32)],
+            4 * share * half * hidden,
+        )(packed, gain, gate, up)
+        state, send = call(
             expert_kernel,
-            [((share, half), bf16)] * 2,
-            12 * share * half * hidden,
-            scratch_shapes=[pltpu.VMEM((share, hidden), bf16)],
-        )(packed, across(packed), ffn_gain.reshape(1, -1), gate, up, down)
-        sums = call(add_kernel, [((span, half), bf16)] * len(turns), 10**6)(keep, across(send))
-        back += [within(value, t) if t else value for t, value in zip(turns, sums)]
-    total, far = call(
-        combine_kernel, [((rows, half), f32), ((rows, half), bf16)], 10**8
-    )(high, low, mid, *back)
-    (updated,) = call(final_kernel, [((rows, half), bf16)], 10**6)(total, opposite(far))
+            [((share, hidden), bf16), ((share, half), bf16)],
+            6 * share * half * hidden,
+        )(across(packed), *partial, gain, gate, up, down)
+        (keep,) = call(keep_kernel, [((share, half), bf16)], 2 * share * half * hidden)(state, down)
+        parts += [keep, across(send)]
+    far, *near = call(
+        add_kernel, [((inner, span, half), bf16)] + [((span, half), bf16)] * inner, 10**6
+    )(*parts)
+    far = returned(far)
+    near = [within(near[t], t) if t else near[t] for t in range(inner)]
+    (sums,) = call(combine_kernel, [((rows, half), bf16)], 10**8)(
+        far_high, far_low, far
+    )
+    (updated,) = call(final_kernel, [((rows, half), bf16)], 10**6)(
+        high, low, mid, opposite(sums), *near
+    )
     return updated, new_state
 
 

time: 74.3 us -> 79 us (1.063)
  blocking collectives: 0 us -> 11.2 us
  waiting for transfers between devices: 35.4 us -> 26 us
  local copies, waits for them, and re-layouts: 0.49 us -> 1.63 us
  starting transfers between devices: 26.3 us -> 27.2 us
  Pallas kernels: 11 us -> 11.8 us
    all_to_all x0 -> x1, blocking collectives: none -> 11.2 us  [returned(): lax.all_to_all(values, 'ep', split_axis=0, concat_axis=0, tiled=True, axi...]
    ppermute x3, waiting for transfers between devices: 15.9 us -> 9.5 us  [opposite(): return lax.ppermute(values, 'ep', [(e, e ^ inner) for e in range(peers)])]
    ppermute x14, waiting for transfers between devices: 18.4 us -> 14.9 us  [within(): return lax.ppermute(values, 'ep', [(e, e ^ t) for e in range(peers)])]
    unnamed x36, local copies, waits for them, and re-layouts: 0.49 us -> 1.63 us
    pallas_call x7 -> x10, Pallas kernels: 8.32 us -> 9.14 us  [the longest x2 3.45 us: local(): call(expert_kernel, [((share, hidden), bf16), ((share, half), bf16)], 6 *...]
  transfers between devices with their start and end apart: 24 -> 24, of which waited for: 14 -> 12; matrix products, arithmetic and copies ran while one was open for 0% -> 0% of each run, Pallas kernels for 8% -> 9%
where the time goes in v1:
time: 79 us; the launch traced here: 78.8 us
  starting transfers between devices  27.2 us (34%)
  waiting for transfers between devices  26 us (33%)
  Pallas kernels  11.8 us (15%)
  blocking collectives  11.2 us (14%)
  local copies, waits for them, and re-layouts  1.63 us (2%)
  between operations  0.96 us (1%)
    ppermute x14, starting transfers between devices, within(): return lax.ppermute(values, 'ep', [(e, e ^ t) for e in range(peers)])  18.5 us
    ppermute x14, waiting for transfers between devices, within(): return lax.ppermute(values, 'ep', [(e, e ^ t) for e in range(peers)])  14.9 us
    all_to_all x1, blocking collectives, returned(): lax.all_to_all(values, 'ep', split_axis=0, concat_axis=0, tiled=True, axi...  11.2 us
    ppermute x3, waiting for transfers between devices, opposite(): return lax.ppermute(values, 'ep', [(e, e ^ inner) for e in range(peers)])  9.5 us
    ppermute x3, starting transfers between devices, opposite(): return lax.ppermute(values, 'ep', [(e, e ^ inner) for e in range(peers)])  7.34 us
    pallas_call x2, Pallas kernels, local(): call(expert_kernel, [((share, hidden), bf16), ((share, half), bf16)], 6 *...  3.45 us
    pallas_call x1, Pallas kernels, local(): call(mixer_kernel, [((rows + 8, channel_half), bf16), (carried_state.shap...  2.62 us
    pallas_call x2, Pallas kernels, local(): call(own_kernel, [((share, hidden), f32)] * 2 + [((share, 128), f32)], 4...  2.03 us
  transfers between devices with their start and end apart: 24, of which 12 were waited for; matrix products, arithmetic and copies ran while one was open for 0% of the time, Pallas kernels for 9%

profile of v1, /device:TPU:0, one launch (start us, length us, event | category | flops | bytes accessed | tf_op | source)
XLA Modules:
  0.0 78.8 jit_solution(6449593250197022271)
XLA Ops:
  0.8 0.6 collective-permute-start
  1.3 1.2 %collective-permute-done.refs_6_ = bf16[64,1024]{1,0:T(8,128)(2,1)S(1)} collective-permute-done((bf16[64,1024]{1,0:T(8,128)(2,1)}, bf16[64,1024]{1,0:T(8,128)(2,1)S(1)}, u32[]{:S(2)}, u32[]{:S(2)}) %collective-permute-start) | collective-permute-done | bytes 131104 | tf_op jit(solution)/shard_map/ppermute | solution.py:352
  2.6 0.1 copy-done.3
  2.7 0.3 copy-done.4
  3.0 2.6 %shard_map.186 = (bf16[72,512]{1,0:T(8,128)(2,1)S(1)}, f32[2,64,2048]{2,1,0:T(8,128)}) custom-call(f32[32,64]{1,0:T(8,128)S(1)} %copy-done.9, f32[32,64]{1,0:T(8,128)S(1)} %copy-done.10, f32[1,32]{1,0:T(1,128)S(1)} %bitcast.34, f32[2,32,16,64]{3,2,1,0:T(8,128)S(1)} %bitcast.25, f32[2,32,16,64]{3,2,1,0:T(8,128)S(1)} %copy-done.6, ...), custom_call_target="tpu_custom_call" | custom-call | flops 1000000000 | bytes 1000000 | tf_op jit(solution)/shard_map/pallas_call | solution.py:387
  5.6 4.1 %collective-permute-start.2 = (bf16[72,512]{1,0:T(8,128)(2,1)S(1)}, bf16[72,512]{1,0:T(8,128)(2,1)S(1)}, u32[]{:S(2)}, u32[]{:S(2)}) collective-permute-start(bf16[72,512]{1,0:T(8,128)(2,1)S(1)} %get-tuple-element.36.own_ref), channel_id=1, source_target_pairs={{0,16},{2,18},{4,20},{6,22},{8,24},{10,26},{12,28},{14,30},{16,0},... | collective-permute-start | bytes 221192 | tf_op jit(solution)/shard_map/ppermute | solution.py:355
  9.7 0.0 collective-permute-start.4
  9.7 6.9 %collective-permute-done.2.far_own_ref = bf16[72,512]{1,0:T(8,128)(2,1)S(1)} collective-permute-done((bf16[72,512]{1,0:T(8,128)(2,1)S(1)}, bf16[72,512]{1,0:T(8,128)(2,1)S(1)}, u32[]{:S(2)}, u32[]{:S(2)}) %collective-permute-start.2) | collective-permute-done | bytes 73760 | tf_op jit(solution)/shard_map/ppermute | solution.py:355
  16.6 0.0 collective-permute-start.3
  16.6 2.6 %collective-permute-done.4.far_residual_ref = bf16[64,1024]{1,0:T(8,128)(2,1)S(1)} collective-permute-done((bf16[64,1024]{1,0:T(8,128)(2,1)S(1)}, bf16[64,1024]{1,0:T(8,128)(2,1)S(1)}, u32[]{:S(2)}, u32[]{:S(2)}) %collective-permute-start.4) | collective-permute-done | bytes 131104 | tf_op jit(solution)/shard_map/ppermute | solution.py:355
  19.2 0.0 collective-permute-done.1.other_ref
  19.2 0.0 collective-permute-done.3.far_other_ref
  19.2 0.0 copy-start
  19.2 0.0 copy-start.1
  19.2 0.0 copy-start.7
  19.2 1.0 %shard_map.187 = (bf16[64,1024]{1,0:T(8,128)(2,1)S(1)}, bf16[192,64]{1,0:T(8,128)(2,1)S(1)}, bf16[192,64]{1,0:T(8,128)(2,1)S(1)}, bf16[192,64]{1,0:T(8,128)(2,1)...) custom-call(bf16[72,512]{1,0:T(8,128)(2,1)S(1)} %get-tuple-element.3, ...), custom_call_target="tpu_custom_call" | custom-call | flops 10000000000 | bytes 1000000 | tf_op jit(solution)/shard_map/pallas_call | solution.py:394
  20.2 0.7 collective-permute-start.10
  21.0 2.5 %collective-permute-start.11 = (bf16[48,1024]{1,0:T(8,128)(2,1)S(1)}, bf16[48,1024]{1,0:T(8,128)(2,1)S(1)}, u32[]{:S(2)}, u32[]{:S(2)}) collective-permute-start(bf16[48,1024]{1,0:T(8,128)(2,1)S(1)} %get-tuple-element.52), channel_id=1, source_target_pairs={{0,10},{2,8},{4,14},{6,12},{8,2},{10,0},{12,6},{14,4},{16,26},{18,... | collective-permute-start | bytes 294920 | tf_op jit(solution)/shard_map/ppermute | solution.py:358
  23.5 1.4 %collective-permute-start.12 = (bf16[48,1024]{1,0:T(8,128)(2,1)S(1)}, bf16[48,1024]{1,0:T(8,128)(2,1)S(1)}, u32[]{:S(2)}, u32[]{:S(2)}) collective-permute-start(bf16[48,1024]{1,0:T(8,128)(2,1)S(1)} %get-tuple-element.53), channel_id=1, source_target_pairs={{0,12},{2,14},{4,8},{6,10},{8,4},{10,6},{12,0},{14,2},{16,28},{18,... | collective-permute-start | bytes 294920 | tf_op jit(solution)/shard_map/ppermute | solution.py:358
  24.9 1.3 %collective-permute-start.13 = (bf16[48,1024]{1,0:T(8,128)(2,1)S(1)}, bf16[48,1024]{1,0:T(8,128)(2,1)S(1)}, u32[]{:S(2)}, u32[]{:S(2)}) collective-permute-start(bf16[48,1024]{1,0:T(8,128)(2,1)S(1)} %get-tuple-element.54), channel_id=1, source_target_pairs={{0,14},{2,12},{4,10},{6,8},{8,6},{10,4},{12,2},{14,0},{16,30},{18,... | collective-permute-start | bytes 294920 | tf_op jit(solution)/shard_map/ppermute | solution.py:358
  26.2 3.1 %collective-permute-done.11.refs_1_ = bf16[48,1024]{1,0:T(8,128)(2,1)S(1)} collective-permute-done((bf16[48,1024]{1,0:T(8,128)(2,1)S(1)}, bf16[48,1024]{1,0:T(8,128)(2,1)S(1)}, u32[]{:S(2)}, u32[]{:S(2)}) %collective-permute-start.11) | collective-permute-done | bytes 98336 | tf_op jit(solution)/shard_map/ppermute | solution.py:358
  29.2 2.0 %collective-permute-done.12.refs_2_ = bf16[48,1024]{1,0:T(8,128)(2,1)S(1)} collective-permute-done((bf16[48,1024]{1,0:T(8,128)(2,1)S(1)}, bf16[48,1024]{1,0:T(8,128)(2,1)S(1)}, u32[]{:S(2)}, u32[]{:S(2)}) %collective-permute-start.12) | collective-permute-done | bytes 98336 | tf_op jit(solution)/shard_map/ppermute | solution.py:358
  31.2 1.8 %collective-permute-done.13.refs_3_ = bf16[48,1024]{1,0:T(8,128)(2,1)S(1)} collective-permute-done((bf16[48,1024]{1,0:T(8,128)(2,1)S(1)}, bf16[48,1024]{1,0:T(8,128)(2,1)S(1)}, u32[]{:S(2)}, u32[]{:S(2)}) %collective-permute-start.13) | collective-permute-done | bytes 98336 | tf_op jit(solution)/shard_map/ppermute | solution.py:358
  33.1 0.1 collective-permute-start.14
  33.2 0.9 %collective-permute-start.5 = (bf16[48,1024]{1,0:T(8,128)(2,1)S(1)}, bf16[48,1024]{1,0:T(8,128)(2,1)S(1)}, u32[]{:S(2)}, u32[]{:S(2)}) collective-permute-start(bf16[48,1024]{1,0:T(8,128)(2,1)S(1)} %get-tuple-element.43), channel_id=1, source_target_pairs={{0,2},{2,0},{4,6},{6,4},{8,10},{10,8},{12,14},{14,12},{16,18},{18,... | collective-permute-start | bytes 294920 | tf_op jit(solution)/shard_map/ppermute | solution.py:358
  34.1 0.4 collective-permute-start.6
  34.5 2.2 %collective-permute-start.7 = (bf16[48,1024]{1,0:T(8,128)(2,1)S(1)}, bf16[48,1024]{1,0:T(8,128)(2,1)S(1)}, u32[]{:S(2)}, u32[]{:S(2)}) collective-permute-start(bf16[48,1024]{1,0:T(8,128)(2,1)S(1)} %get-tuple-element.45), channel_id=1, source_target_pairs={{0,6},{2,4},{4,2},{6,0},{8,14},{10,12},{12,10},{14,8},{16,22},{18,... | collective-permute-start | bytes 294920 | tf_op jit(solution)/shard_map/ppermute | solution.py:358
  36.7 2.0 %collective-permute-done.5.refs_1_ = bf16[48,1024]{1,0:T(8,128)(2,1)S(1)} collective-permute-done((bf16[48,1024]{1,0:T(8,128)(2,1)S(1)}, bf16[48,1024]{1,0:T(8,128)(2,1)S(1)}, u32[]{:S(2)}, u32[]{:S(2)}) %collective-permute-start.5) | collective-permute-done | bytes 98336 | tf_op jit(solution)/shard_map/ppermute | solution.py:358
  38.7 2.4 %collective-permute-done.6.refs_2_ = bf16[48,1024]{1,0:T(8,128)(2,1)S(1)} collective-permute-done((bf16[48,1024]{1,0:T(8,128)(2,1)S(1)}, bf16[48,1024]{1,0:T(8,128)(2,1)S(1)}, u32[]{:S(2)}, u32[]{:S(2)}) %collective-permute-start.6) | collective-permute-done | bytes 98336 | tf_op jit(solution)/shard_map/ppermute | solution.py:358
  41.1 0.0 collective-permute-done.7.refs_3_
  41.1 0.1 collective-permute-start.8
  41.2 1.0 %shard_map.193 = (f32[192,1024]{1,0:T(8,128)S(1)}, f32[192,1024]{1,0:T(8,128)S(1)}, f32[192,128]{1,0:T(8,128)S(1)}) custom-call(bf16[192,1024]{1,0:T(8,128)(2,1)S(1)} %shard_map.192.own_ref, f32[1,2048]{1,0:T(1,128)S(1)} %bitcast.26, bf16[2048,1024]{1,0:T(8,128)(2,1)S(1)} %bitcast.12, bf16[2048,1024]{1,0:T(8,128)(2,1)S(1)} %bitcast.16), custom_call_target="tpu_custom_call" | custom-call | flops 805306368 | bytes 1000000 | tf_op jit(solution)/shard_map/pallas_call | solution.py:417
  42.2 0.0 copy-start.2
  42.3 1.0 %shard_map.189 = (f32[192,1024]{1,0:T(8,128)S(1)}, f32[192,1024]{1,0:T(8,128)S(1)}, f32[192,128]{1,0:T(8,128)S(1)}) custom-call(bf16[192,1024]{1,0:T(8,128)(2,1)S(1)} %shard_map.188.own_ref, f32[1,2048]{1,0:T(1,128)S(1)} %bitcast.27, bf16[2048,1024]{1,0:T(8,128)(2,1)S(1)} %bitcast.13, bf16[2048,1024]{1,0:T(8,128)(2,1)S(1)} %bitcast.17), custom_call_target="tpu_custom_call" | custom-call | flops 805306368 | bytes 1000000 | tf_op jit(solution)/shard_map/pallas_call | solution.py:417
  43.3 0.0 collective-permute-done.14.other_ref
  43.3 1.1 %copy-done.2 = bf16[1,1024,2048]{2,1,0:T(8,128)(2,1)S(1)} copy-done((bf16[1,1024,2048]{2,1,0:T(8,128)(2,1)S(1)}, bf16[1,1024,2048]{2,1,0:T(8,128)(2,1)}, u32[]{:S(2)}) %copy-start.2) | copy-done | bytes 4194328
  44.4 1.7 %shard_map.194 = (bf16[192,1024]{1,0:T(8,128)(2,1)S(1)}, bf16[192,1024]{1,0:T(8,128)(2,1)S(1)}) custom-call(bf16[192,1024]{1,0:T(8,128)(2,1)S(1)} %collective-permute-done.14.other_ref, f32[192,1024]{1,0:T(8,128)S(1)} %get-tuple-element.55.gate_sum_ref, f32[192,1024]{1,0:T(8,128)S(1)} %get-tuple-element.56.up_sum_ref, ...), custom_call_target="tpu_custom_call" | custom-call | flops 1207959552 | bytes 1000000 | tf_op jit(solution)/shard_map/pallas_call | solution.py:422
  46.2 0.5 collective-permute-start.15
  46.7 0.0 collective-permute-done.8.other_ref
  46.7 1.7 %shard_map.190 = (bf16[192,1024]{1,0:T(8,128)(2,1)S(1)}, bf16[192,1024]{1,0:T(8,128)(2,1)S(1)}) custom-call(bf16[192,1024]{1,0:T(8,128)(2,1)S(1)} %collective-permute-done.8.other_ref, f32[192,1024]{1,0:T(8,128)S(1)} %get-tuple-element.46.gate_sum_ref, f32[192,1024]{1,0:T(8,128)S(1)} %get-tuple-element.47.up_sum_ref, ...), custom_call_target="tpu_custom_call" | custom-call | flops 1207959552 | bytes 1000000 | tf_op jit(solution)/shard_map/pallas_call | solution.py:422
  48.4 0.1 collective-permute-start.9
  48.6 0.6 shard_map.195.refs_2_
  49.2 0.6 shard_map.191.refs_0_
  49.8 0.0 collective-permute-done.15.refs_3_
  49.8 0.4 collective-permute-done.9.refs_1_
  50.2 0.2 shard_map.196
  50.4 11.2 %all_to_all.5 = bf16[8,24,1024]{2,1,0:T(8,128)(2,1)S(1)} all-to-all(bf16[8,24,1024]{2,1,0:T(8,128)(2,1)S(1)} %get-tuple-element.60), channel_id=1, replica_groups={{0,2,4,6,8,10,12,14},{16,18,20,22,24,26,28,30},{1,3,5,7,9,11,13,15},{17..., dimensions={0} | all-to-all | bytes 786432 | tf_op jit(solution)/shard_map/all_to_all | solution.py:363
  61.6 0.3 shard_map.197
  61.9 3.2 %collective-permute-start.16 = (bf16[64,1024]{1,0:T(8,128)(2,1)S(1)}, bf16[64,1024]{1,0:T(8,128)(2,1)S(1)}, u32[]{:S(2)}, u32[]{:S(2)}) collective-permute-start(bf16[64,1024]{1,0:T(8,128)(2,1)S(1)} %shard_map.197), channel_id=1, source_target_pairs={{0,16},{2,18},{4,20},{6,22},{8,24},{10,26},{12,28},{14,30},{16,0},... | collective-permute-start | bytes 393224 | tf_op jit(solution)/shard_map/ppermute | solution.py:355
  65.1 0.4 collective-permute-start.17
  65.5 0.9 %collective-permute-start.18 = (bf16[24,1024]{1,0:T(8,128)(2,1)S(1)}, bf16[24,1024]{1,0:T(8,128)(2,1)S(1)}, u32[]{:S(2)}, u32[]{:S(2)}) collective-permute-start(bf16[24,1024]{1,0:T(8,128)(2,1)S(1)} %get-tuple-element.63), channel_id=1, source_target_pairs={{0,4},{2,6},{4,0},{6,2},{8,12},{10,14},{12,8},{14,10},{16,20},{18,... | collective-permute-start | bytes 147464 | tf_op jit(solution)/shard_map/ppermute | solution.py:358
  66.4 2.2 %collective-permute-start.19 = (bf16[24,1024]{1,0:T(8,128)(2,1)S(1)}, bf16[24,1024]{1,0:T(8,128)(2,1)S(1)}, u32[]{:S(2)}, u32[]{:S(2)}) collective-permute-start(bf16[24,1024]{1,0:T(8,128)(2,1)S(1)} %get-tuple-element.64), channel_id=1, source_target_pairs={{0,6},{2,4},{4,2},{6,0},{8,14},{10,12},{12,10},{14,8},{16,22},{18,... | collective-permute-start | bytes 147464 | tf_op jit(solution)/shard_map/ppermute | solution.py:358
  68.6 0.7 collective-permute-start.20
  69.4 0.0 collective-permute-done.17.refs_1_
  69.4 1.1 %collective-permute-start.21 = (bf16[24,1024]{1,0:T(8,128)(2,1)S(1)}, bf16[24,1024]{1,0:T(8,128)(2,1)S(1)}, u32[]{:S(2)}, u32[]{:S(2)}) collective-permute-start(bf16[24,1024]{1,0:T(8,128)(2,1)S(1)} %get-tuple-element.66), channel_id=1, source_target_pairs={{0,10},{2,8},{4,14},{6,12},{8,2},{10,0},{12,6},{14,4},{16,26},{18,... | collective-permute-start | bytes 147464 | tf_op jit(solution)/shard_map/ppermute | solution.py:358
  70.5 0.0 collective-permute-done.18.refs_2_
  70.5 1.2 %collective-permute-start.22 = (bf16[24,1024]{1,0:T(8,128)(2,1)S(1)}, bf16[24,1024]{1,0:T(8,128)(2,1)S(1)}, u32[]{:S(2)}, u32[]{:S(2)}) collective-permute-start(bf16[24,1024]{1,0:T(8,128)(2,1)S(1)} %get-tuple-element.67), channel_id=1, source_target_pairs={{0,12},{2,14},{4,8},{6,10},{8,4},{10,6},{12,0},{14,2},{16,28},{18,... | collective-permute-start | bytes 147464 | tf_op jit(solution)/shard_map/ppermute | solution.py:358
  71.7 0.3 collective-permute-done.19.refs_3_
  72.0 2.5 %collective-permute-start.23 = (bf16[24,1024]{1,0:T(8,128)(2,1)S(1)}, bf16[24,1024]{1,0:T(8,128)(2,1)S(1)}, u32[]{:S(2)}, u32[]{:S(2)}) collective-permute-start(bf16[24,1024]{1,0:T(8,128)(2,1)S(1)} %get-tuple-element.68), channel_id=1, source_target_pairs={{0,14},{2,12},{4,10},{6,8},{8,6},{10,4},{12,2},{14,0},{16,30},{18,... | collective-permute-start | bytes 147464 | tf_op jit(solution)/shard_map/ppermute | solution.py:358
  74.5 0.0 collective-permute-done.20.refs_4_
  74.5 0.0 collective-permute-done.21.refs_5_
  74.5 1.0 %collective-permute-done.22.refs_6_ = bf16[24,1024]{1,0:T(8,128)(2,1)S(1)} collective-permute-done((bf16[24,1024]{1,0:T(8,128)(2,1)S(1)}, bf16[24,1024]{1,0:T(8,128)(2,1)S(1)}, u32[]{:S(2)}, u32[]{:S(2)}) %collective-permute-start.22) | collective-permute-done | bytes 49184 | tf_op jit(solution)/shard_map/ppermute | solution.py:358
  75.5 2.4 %collective-permute-done.23.refs_7_ = bf16[24,1024]{1,0:T(8,128)(2,1)S(1)} collective-permute-done((bf16[24,1024]{1,0:T(8,128)(2,1)S(1)}, bf16[24,1024]{1,0:T(8,128)(2,1)S(1)}, u32[]{:S(2)}, u32[]{:S(2)}) %collective-permute-start.23) | collective-permute-done | bytes 49184 | tf_op jit(solution)/shard_map/ppermute | solution.py:358
  77.9 0.9 %shard_map.198 = bf16[64,1024]{1,0:T(8,128)(2,1)} custom-call(bf16[192,64]{1,0:T(8,128)(2,1)S(1)} %get-tuple-element.37.high_ref, bf16[192,64]{1,0:T(8,128)(2,1)S(1)} %get-tuple-element.38.low_ref, bf16[64,1024]{1,0:T(8,128)(2,1)S(1)} %get-tuple-element.39.mid_ref, bf16[64,1024]{1,0:T(8,128)(2,1)S(1)} %collective-permute-done.16.far_ref, ...), custom_call_target="tpu_custom_call" | custom-call | flops 1000000 | bytes 1000000 | tf_op jit(solution)/shard_map/pallas_call | solution.py:437
  (35 shorter events, 0.1 us)
Async XLA Ops:
  0.6 1.9 %copy-start.8 = (bf16[64,1024]{1,0:T(8,128)(2,1)S(1)}, bf16[64,1024]{1,0:T(8,128)(2,1)}, u32[]{:S(2)}) copy-start(bf16[64,1024]{1,0:T(8,128)(2,1)} %residual_ref.1) | copy-start | bytes 393220
  0.6 1.9 %copy-start.12 = (f32[512]{0:T(512)S(1)}, f32[512]{0:T(512)}, u32[]{:S(2)}) copy-start(f32[512]{0:T(512)} %param.29) | copy-start | bytes 6148
  0.7 1.9 %copy-start.6 = (f32[2,32,16,64]{3,2,1,0:T(8,128)S(1)}, f32[2,32,16,64]{3,2,1,0:T(8,128)}, u32[]{:S(2)}) copy-start(f32[2,32,16,64]{3,2,1,0:T(8,128)} %refs_4_.1) | copy-start | bytes 786436
  0.7 1.9 %copy-start.5 = (f32[2,32,64,16]{2,3,1,0:T(8,128)S(1)}, f32[2,32,64,16]{2,3,1,0:T(8,128)}, u32[]{:S(2)}) copy-start(f32[2,32,64,16]{2,3,1,0:T(8,128)} %param.27) | copy-start | bytes 786436
  0.7 1.9 %copy-start.15 = (f32[32]{0:T(128)S(1)}, f32[32]{0:T(128)}, u32[]{:S(2)}) copy-start(f32[32]{0:T(128)} %param.26) | copy-start | bytes 388
  0.7 1.9 %copy-start.10 = (f32[32,64]{1,0:T(8,128)S(1)}, f32[32,64]{1,0:T(8,128)}, u32[]{:S(2)}) copy-start(f32[32,64]{1,0:T(8,128)} %refs_1_.1) | copy-start | bytes 24580
  0.7 1.9 %copy-start.9 = (f32[32,64]{1,0:T(8,128)S(1)}, f32[32,64]{1,0:T(8,128)}, u32[]{:S(2)}) copy-start(f32[32,64]{1,0:T(8,128)} %refs_0_.1) | copy-start | bytes 24580
  0.7 2.0 %copy-start.3 = (bf16[2048,512]{1,0:T(8,128)(2,1)S(1)}, bf16[2048,512]{1,0:T(8,128)(2,1)}, u32[]{:S(2)}) copy-start(bf16[2048,512]{1,0:T(8,128)(2,1)} %refs_8_.1) | copy-start | bytes 6291460
  0.7 2.0 %copy-start.11 = (f32[2048]{0:T(1024)S(1)}, f32[2048]{0:T(1024)}, u32[]{:S(2)}) copy-start(f32[2048]{0:T(1024)} %param.22) | copy-start | bytes 24580
  0.7 2.2 %copy-start.4 = (f32[2,64,2048]{2,1,0:T(8,128)S(1)}, f32[2,64,2048]{2,1,0:T(8,128)}, u32[]{:S(2)}) copy-start(f32[2,64,2048]{2,1,0:T(8,128)} %refs_12_.1) | copy-start | bytes 3145732
  0.7 2.2 %copy-start.14 = (f32[64,4]{0,1:T(4,128)S(1)}, f32[64,4]{0,1:T(4,128)}, u32[]{:S(2)}) copy-start(f32[64,4]{0,1:T(4,128)} %param.20) | copy-start | bytes 3076
  0.7 2.2 %copy-start.13 = (s32[64,4]{0,1:T(4,128)S(1)}, s32[64,4]{0,1:T(4,128)}, u32[]{:S(2)}) copy-start(s32[64,4]{0,1:T(4,128)} %param.19) | copy-start | bytes 3076
  0.8 1.8 %collective-permute-start = (bf16[64,1024]{1,0:T(8,128)(2,1)}, bf16[64,1024]{1,0:T(8,128)(2,1)S(1)}, u32[]{:S(2)}, u32[]{:S(2)}) collective-permute-start(bf16[64,1024]{1,0:T(8,128)(2,1)} %residual_ref.1), channel_id=1, source_target_pairs={{0,1},{1,0},{2,3},{3,2},{4,5},{5,4},{6,7},{7,6},{8,9},{9,8},{10,11... | collective-permute-start | bytes 393224 | tf_op jit(solution)/shard_map/ppermute | solution.py:352
  1.3 17.9 %copy-start.16 = (bf16[1024,1024]{1,0:T(8,128)(2,1)S(1)}, bf16[1024,1024]{1,0:T(8,128)(2,1)}, u32[]{:S(2)}) copy-start(bf16[1024,1024]{1,0:T(8,128)(2,1)} %proj_ref.1) | copy-start | bytes 6291460
  1.3 17.9 %copy-start.17 = (f32[1024]{0:T(1024)S(1)}, f32[1024]{0:T(1024)}, u32[]{:S(2)}) copy-start(f32[1024]{0:T(1024)} %param.30) | copy-start | bytes 12292
  5.6 11.0 %collective-permute-start.2 = (bf16[72,512]{1,0:T(8,128)(2,1)S(1)}, bf16[72,512]{1,0:T(8,128)(2,1)S(1)}, u32[]{:S(2)}, u32[]{:S(2)}) collective-permute-start(bf16[72,512]{1,0:T(8,128)(2,1)S(1)} %get-tuple-element.36.own_ref), channel_id=1, source_target_pairs={{0,16},{2,18},{4,20},{6,22},{8,24},{10,26},{12,28},{14,30},{16,0},... | collective-permute-start | bytes 221192 | tf_op jit(solution)/shard_map/ppermute | solution.py:355
  9.7 9.5 %collective-permute-start.4 = (bf16[64,1024]{1,0:T(8,128)(2,1)S(1)}, bf16[64,1024]{1,0:T(8,128)(2,1)S(1)}, u32[]{:S(2)}, u32[]{:S(2)}) collective-permute-start(bf16[64,1024]{1,0:T(8,128)(2,1)S(1)} %copy-done.8), channel_id=1, source_target_pairs={{0,16},{2,18},{4,20},{6,22},{8,24},{10,26},{12,28},{14,30},{16,0},... | collective-permute-start | bytes 393224 | tf_op jit(solution)/shard_map/ppermute | solution.py:355
  9.7 9.5 %collective-permute-start.1 = (bf16[72,512]{1,0:T(8,128)(2,1)S(1)}, bf16[72,512]{1,0:T(8,128)(2,1)S(1)}, u32[]{:S(2)}, u32[]{:S(2)}) collective-permute-start(bf16[72,512]{1,0:T(8,128)(2,1)S(1)} %get-tuple-element.36.own_ref), channel_id=1, source_target_pairs={{0,1},{1,0},{2,3},{3,2},{4,5},{5,4},{6,7},{7,6},{8,9},{9,8},{10,11... | collective-permute-start | bytes 221192 | tf_op jit(solution)/shard_map/ppermute | solution.py:352
  16.6 2.6 %collective-permute-start.3 = (bf16[72,512]{1,0:T(8,128)(2,1)S(1)}, bf16[72,512]{1,0:T(8,128)(2,1)S(1)}, u32[]{:S(2)}, u32[]{:S(2)}) collective-permute-start(bf16[72,512]{1,0:T(8,128)(2,1)S(1)} %collective-permute-done.2.far_own_ref), channel_id=1, source_target_pairs={{0,1},{1,0},{2,3},{3,2},{4,5},{5,4},{6,7},{7,6},{8,9},{9,8},{10,11... | collective-permute-start | bytes 221192 | tf_op jit(solution)/shard_map/ppermute | solution.py:352
  19.2 22.0 %copy-start = (bf16[1,2048,1024]{2,1,0:T(8,128)(2,1)S(1)}, bf16[1,2048,1024]{2,1,0:T(8,128)(2,1)}, u32[]{:S(2)}) copy-start(bf16[1,2048,1024]{2,1,0:T(8,128)(2,1)} %param.33) | copy-start | bytes 12582916
  19.2 22.0 %copy-start.1 = (bf16[1,2048,1024]{2,1,0:T(8,128)(2,1)S(1)}, bf16[1,2048,1024]{2,1,0:T(8,128)(2,1)}, u32[]{:S(2)}) copy-start(bf16[1,2048,1024]{2,1,0:T(8,128)(2,1)} %param.34) | copy-start | bytes 12582916
  19.2 22.0 %copy-start.7 = (f32[2048]{0:T(1024)S(1)}, f32[2048]{0:T(1024)}, u32[]{:S(2)}) copy-start(f32[2048]{0:T(1024)} %param.32) | copy-start | bytes 24580
  20.2 5.9 %collective-permute-start.10 = (bf16[48,1024]{1,0:T(8,128)(2,1)S(1)}, bf16[48,1024]{1,0:T(8,128)(2,1)S(1)}, u32[]{:S(2)}, u32[]{:S(2)}) collective-permute-start(bf16[48,1024]{1,0:T(8,128)(2,1)S(1)} %get-tuple-element.51), channel_id=1, source_target_pairs={{0,8},{2,10},{4,12},{6,14},{8,0},{10,2},{12,4},{14,6},{16,24},{18,... | collective-permute-start | bytes 294920 | tf_op jit(solution)/shard_map/ppermute | solution.py:358
  21.0 8.2 %collective-permute-start.11 = (bf16[48,1024]{1,0:T(8,128)(2,1)S(1)}, bf16[48,1024]{1,0:T(8,128)(2,1)S(1)}, u32[]{:S(2)}, u32[]{:S(2)}) collective-permute-start(bf16[48,1024]{1,0:T(8,128)(2,1)S(1)} %get-tuple-element.52), channel_id=1, source_target_pairs={{0,10},{2,8},{4,14},{6,12},{8,2},{10,0},{12,6},{14,4},{16,26},{18,... | collective-permute-start | bytes 294920 | tf_op jit(solution)/shard_map/ppermute | solution.py:358
  23.5 7.8 %collective-permute-start.12 = (bf16[48,1024]{1,0:T(8,128)(2,1)S(1)}, bf16[48,1024]{1,0:T(8,128)(2,1)S(1)}, u32[]{:S(2)}, u32[]{:S(2)}) collective-permute-start(bf16[48,1024]{1,0:T(8,128)(2,1)S(1)} %get-tuple-element.53), channel_id=1, source_target_pairs={{0,12},{2,14},{4,8},{6,10},{8,4},{10,6},{12,0},{14,2},{16,28},{18,... | collective-permute-start | bytes 294920 | tf_op jit(solution)/shard_map/ppermute | solution.py:358
  24.9 8.2 %collective-permute-start.13 = (bf16[48,1024]{1,0:T(8,128)(2,1)S(1)}, bf16[48,1024]{1,0:T(8,128)(2,1)S(1)}, u32[]{:S(2)}, u32[]{:S(2)}) collective-permute-start(bf16[48,1024]{1,0:T(8,128)(2,1)S(1)} %get-tuple-element.54), channel_id=1, source_target_pairs={{0,14},{2,12},{4,10},{6,8},{8,6},{10,4},{12,2},{14,0},{16,30},{18,... | collective-permute-start | bytes 294920 | tf_op jit(solution)/shard_map/ppermute | solution.py:358
  33.1 10.2 %collective-permute-start.14 = (bf16[192,1024]{1,0:T(8,128)(2,1)S(1)}, bf16[192,1024]{1,0:T(8,128)(2,1)S(1)}, u32[]{:S(2)}, u32[]{:S(2)}) collective-permute-start(bf16[192,1024]{1,0:T(8,128)(2,1)S(1)} %shard_map.192.own_ref), channel_id=1, source_target_pairs={{0,1},{1,0},{2,3},{3,2},{4,5},{5,4},{6,7},{7,6},{8,9},{9,8},{10,11... | collective-permute-start | bytes 1179656 | tf_op jit(solution)/shard_map/ppermute | solution.py:352
  33.2 5.5 %collective-permute-start.5 = (bf16[48,1024]{1,0:T(8,128)(2,1)S(1)}, bf16[48,1024]{1,0:T(8,128)(2,1)S(1)}, u32[]{:S(2)}, u32[]{:S(2)}) collective-permute-start(bf16[48,1024]{1,0:T(8,128)(2,1)S(1)} %get-tuple-element.43), channel_id=1, source_target_pairs={{0,2},{2,0},{4,6},{6,4},{8,10},{10,8},{12,14},{14,12},{16,18},{18,... | collective-permute-start | bytes 294920 | tf_op jit(solution)/shard_map/ppermute | solution.py:358
  34.1 7.0 %collective-permute-start.6 = (bf16[48,1024]{1,0:T(8,128)(2,1)S(1)}, bf16[48,1024]{1,0:T(8,128)(2,1)S(1)}, u32[]{:S(2)}, u32[]{:S(2)}) collective-permute-start(bf16[48,1024]{1,0:T(8,128)(2,1)S(1)} %get-tuple-element.44), channel_id=1, source_target_pairs={{0,4},{2,6},{4,0},{6,2},{8,12},{10,14},{12,8},{14,10},{16,20},{18,... | collective-permute-start | bytes 294920 | tf_op jit(solution)/shard_map/ppermute | solution.py:358
  34.5 6.6 %collective-permute-start.7 = (bf16[48,1024]{1,0:T(8,128)(2,1)S(1)}, bf16[48,1024]{1,0:T(8,128)(2,1)S(1)}, u32[]{:S(2)}, u32[]{:S(2)}) collective-permute-start(bf16[48,1024]{1,0:T(8,128)(2,1)S(1)} %get-tuple-element.45), channel_id=1, source_target_pairs={{0,6},{2,4},{4,2},{6,0},{8,14},{10,12},{12,10},{14,8},{16,22},{18,... | collective-permute-start | bytes 294920 | tf_op jit(solution)/shard_map/ppermute | solution.py:358
  41.1 5.6 %collective-permute-start.8 = (bf16[192,1024]{1,0:T(8,128)(2,1)S(1)}, bf16[192,1024]{1,0:T(8,128)(2,1)S(1)}, u32[]{:S(2)}, u32[]{:S(2)}) collective-permute-start(bf16[192,1024]{1,0:T(8,128)(2,1)S(1)} %shard_map.188.own_ref), channel_id=1, source_target_pairs={{0,1},{1,0},{2,3},{3,2},{4,5},{5,4},{6,7},{7,6},{8,9},{9,8},{10,11... | collective-permute-start | bytes 1179656 | tf_op jit(solution)/shard_map/ppermute | solution.py:352
  42.2 2.2 %copy-start.2 = (bf16[1,1024,2048]{2,1,0:T(8,128)(2,1)S(1)}, bf16[1,1024,2048]{2,1,0:T(8,128)(2,1)}, u32[]{:S(2)}) copy-start(bf16[1,1024,2048]{2,1,0:T(8,128)(2,1)} %param.35) | copy-start | bytes 12582916
  46.2 3.7 %collective-permute-start.15 = (bf16[192,1024]{1,0:T(8,128)(2,1)S(1)}, bf16[192,1024]{1,0:T(8,128)(2,1)S(1)}, u32[]{:S(2)}, u32[]{:S(2)}) collective-permute-start(bf16[192,1024]{1,0:T(8,128)(2,1)S(1)} %get-tuple-element.59), channel_id=1, source_target_pairs={{0,1},{1,0},{2,3},{3,2},{4,5},{5,4},{6,7},{7,6},{8,9},{9,8},{10,11... | collective-permute-start | bytes 1179656 | tf_op jit(solution)/shard_map/ppermute | solution.py:352
  48.4 1.8 %collective-permute-start.9 = (bf16[192,1024]{1,0:T(8,128)(2,1)S(1)}, bf16[192,1024]{1,0:T(8,128)(2,1)S(1)}, u32[]{:S(2)}, u32[]{:S(2)}) collective-permute-start(bf16[192,1024]{1,0:T(8,128)(2,1)S(1)} %get-tuple-element.50), channel_id=1, source_target_pairs={{0,1},{1,0},{2,3},{3,2},{4,5},{5,4},{6,7},{7,6},{8,9},{9,8},{10,11... | collective-permute-start | bytes 1179656 | tf_op jit(solution)/shard_map/ppermute | solution.py:352
  61.9 16.0 %collective-permute-start.16 = (bf16[64,1024]{1,0:T(8,128)(2,1)S(1)}, bf16[64,1024]{1,0:T(8,128)(2,1)S(1)}, u32[]{:S(2)}, u32[]{:S(2)}) collective-permute-start(bf16[64,1024]{1,0:T(8,128)(2,1)S(1)} %shard_map.197), channel_id=1, source_target_pairs={{0,16},{2,18},{4,20},{6,22},{8,24},{10,26},{12,28},{14,30},{16,0},... | collective-permute-start | bytes 393224 | tf_op jit(solution)/shard_map/ppermute | solution.py:355
  65.1 4.2 %collective-permute-start.17 = (bf16[24,1024]{1,0:T(8,128)(2,1)S(1)}, bf16[24,1024]{1,0:T(8,128)(2,1)S(1)}, u32[]{:S(2)}, u32[]{:S(2)}) collective-permute-start(bf16[24,1024]{1,0:T(8,128)(2,1)S(1)} %get-tuple-element.62), channel_id=1, source_target_pairs={{0,2},{2,0},{4,6},{6,4},{8,10},{10,8},{12,14},{14,12},{16,18},{18,... | collective-permute-start | bytes 147464 | tf_op jit(solution)/shard_map/ppermute | solution.py:358
  65.5 5.0 %collective-permute-start.18 = (bf16[24,1024]{1,0:T(8,128)(2,1)S(1)}, bf16[24,1024]{1,0:T(8,128)(2,1)S(1)}, u32[]{:S(2)}, u32[]{:S(2)}) collective-permute-start(bf16[24,1024]{1,0:T(8,128)(2,1)S(1)} %get-tuple-element.63), channel_id=1, source_target_pairs={{0,4},{2,6},{4,0},{6,2},{8,12},{10,14},{12,8},{14,10},{16,20},{18,... | collective-permute-start | bytes 147464 | tf_op jit(solution)/shard_map/ppermute | solution.py:358
  66.4 5.5 %collective-permute-start.19 = (bf16[24,1024]{1,0:T(8,128)(2,1)S(1)}, bf16[24,1024]{1,0:T(8,128)(2,1)S(1)}, u32[]{:S(2)}, u32[]{:S(2)}) collective-permute-start(bf16[24,1024]{1,0:T(8,128)(2,1)S(1)} %get-tuple-element.64), channel_id=1, source_target_pairs={{0,6},{2,4},{4,2},{6,0},{8,14},{10,12},{12,10},{14,8},{16,22},{18,... | collective-permute-start | bytes 147464 | tf_op jit(solution)/shard_map/ppermute | solution.py:358
  68.6 5.9 %collective-permute-start.20 = (bf16[24,1024]{1,0:T(8,128)(2,1)S(1)}, bf16[24,1024]{1,0:T(8,128)(2,1)S(1)}, u32[]{:S(2)}, u32[]{:S(2)}) collective-permute-start(bf16[24,1024]{1,0:T(8,128)(2,1)S(1)} %get-tuple-element.65), channel_id=1, source_target_pairs={{0,8},{2,10},{4,12},{6,14},{8,0},{10,2},{12,4},{14,6},{16,24},{18,... | collective-permute-start | bytes 147464 | tf_op jit(solution)/shard_map/ppermute | solution.py:358
  69.4 5.1 %collective-permute-start.21 = (bf16[24,1024]{1,0:T(8,128)(2,1)S(1)}, bf16[24,1024]{1,0:T(8,128)(2,1)S(1)}, u32[]{:S(2)}, u32[]{:S(2)}) collective-permute-start(bf16[24,1024]{1,0:T(8,128)(2,1)S(1)} %get-tuple-element.66), channel_id=1, source_target_pairs={{0,10},{2,8},{4,14},{6,12},{8,2},{10,0},{12,6},{14,4},{16,26},{18,... | collective-permute-start | bytes 147464 | tf_op jit(solution)/shard_map/ppermute | solution.py:358
  70.5 5.0 %collective-permute-start.22 = (bf16[24,1024]{1,0:T(8,128)(2,1)S(1)}, bf16[24,1024]{1,0:T(8,128)(2,1)S(1)}, u32[]{:S(2)}, u32[]{:S(2)}) collective-permute-start(bf16[24,1024]{1,0:T(8,128)(2,1)S(1)} %get-tuple-element.67), channel_id=1, source_target_pairs={{0,12},{2,14},{4,8},{6,10},{8,4},{10,6},{12,0},{14,2},{16,28},{18,... | collective-permute-start | bytes 147464 | tf_op jit(solution)/shard_map/ppermute | solution.py:358
  72.0 5.9 %collective-permute-start.23 = (bf16[24,1024]{1,0:T(8,128)(2,1)S(1)}, bf16[24,1024]{1,0:T(8,128)(2,1)S(1)}, u32[]{:S(2)}, u32[]{:S(2)}) collective-permute-start(bf16[24,1024]{1,0:T(8,128)(2,1)S(1)} %get-tuple-element.68), channel_id=1, source_target_pairs={{0,14},{2,12},{4,10},{6,8},{8,6},{10,4},{12,2},{14,0},{16,30},{18,... | collective-permute-start | bytes 147464 | tf_op jit(solution)/shard_map/ppermute | solution.py:358

commit v2 on v1

--- a/solution.py
+++ b/solution.py
@@ -17,6 +17,7 @@
 TN = (((0,), (0,)), ((), ()))
 MIXER_VMEM = 16
 HEAD_FLOPS = 10**11
+PREPARE_VMEM = 12
 
 
 def mm(a, b, dims=NN):
@@ -50,10 +51,10 @@
     out_ref[...] = jnp.zeros_like(out_ref)
 
 
-def mixer_kernel(*refs):
-    decay_ref, freq_ref, step_ref, map_ref, out_ref, own_ref, other_ref, gain_ref = refs[:8]
-    proj_ref, skip_ref, ids_ref, weights_ref, state_ref, _, act_ref, new_ref = refs[8:]
-    groups, width = decay_ref.shape
+def prepare_kernel(
+    decay_ref, freq_ref, step_ref, map_ref, out_ref, _, bars_ref, tables_ref
+):
+    groups, _ = decay_ref.shape
     per_group = map_ref.shape[2]
     step = step_ref[...]
     square = jnp.broadcast_to(step, (groups, groups))
@@ -71,26 +72,34 @@
     coef_imag = ((bar_imag * rate - shifted * freq) * inverse)[:, None, :]
     map_real = coef_real * map_ref[0] - coef_imag * map_ref[1]
     map_imag = coef_real * map_ref[1] + coef_imag * map_ref[0]
-    bar_real, bar_imag = flat_row(bar_real), flat_row(bar_imag)
-    count = max(1, min(groups, 128 // per_group))
-    blocks = [slice(i * count, (i + 1) * count) for i in range(groups // count)]
-    tables = [
-        split(spread(map_real[held], count))
-        + split(spread(map_imag[held], count))
-        + (spread(out_ref[0, held], count).astype(bf16), spread(-out_ref[1, held], count).astype(bf16))
-        for held in blocks
-    ]
+    bars_ref[...] = jnp.concatenate([flat_row(bar_real), flat_row(bar_imag)], axis=0)
+    count = tables_ref.shape[2] // per_group
+    for i in range(groups // count):
+        held = slice(i * count, (i + 1) * count)
+        parts = split(spread(map_real[held], count)) + split(spread(map_imag[held], count))
+        for k, part in enumerate(parts):
+            tables_ref[i, k] = part
+        tables_ref[i, 4] = spread(out_ref[0, held], count).astype(bf16)
+        tables_ref[i, 5] = spread(-out_ref[1, held], count).astype(bf16)
+
+
+def mixer_kernel(*refs):
+    bars_ref, tables_ref, own_ref, other_ref, gain_ref, proj_ref, skip_ref = refs[:7]
+    ids_ref, weights_ref, state_ref, act_ref, new_ref = refs[7:]
     low, high = normed(own_ref[...], other_ref[...], gain_ref[...], lax.axis_index("tp") == 0)
     half = low.shape[1]
     channels = (mm(low, proj_ref[:half, :]) + mm(high, proj_ref[half:, :])).astype(bf16)
     rows = low.shape[0]
-    lanes, columns = count * width, count * per_group
-    for block, (real_high, real_low, imag_high, imag_low, out_real, out_imag) in enumerate(tables):
+    blocks, _, columns, lanes = tables_ref.shape
+    for block in range(blocks):
+        real_high, real_low, imag_high, imag_low, out_real, out_imag = (
+            tables_ref[block, k] for k in range(6)
+        )
         wide = slice(block * lanes, (block + 1) * lanes)
         narrow = slice(block * columns, (block + 1) * columns)
         fed = channels[:, narrow]
         old_real, old_imag = state_ref[0, :, wide], state_ref[1, :, wide]
-        turn_real, turn_imag = bar_real[:, wide], bar_imag[:, wide]
+        turn_real, turn_imag = bars_ref[:1, wide], bars_ref[1:, wide]
         next_real = (
             turn_real * old_real - turn_imag * old_imag + (mm(fed, real_high) + mm(fed, real_low))
         )
@@ -214,6 +223,10 @@
         ref[...] = sent[2 * t * span : 2 * (t + 1) * span].astype(bf16)
 
 
+def store_kernel(value_ref, out_ref):
+    out_ref[...] = value_ref[...]
+
+
 def pack_kernel(*refs):
     refs[-1][...] = jnp.concatenate([ref[...] for ref in refs[:-1]], axis=0)
 
@@ -226,7 +239,7 @@
     return (values * gain_ref[:, part]).astype(bf16), total, part
 
 
-def own_kernel(own_ref, gain_ref, gate_ref, up_ref, gate_sum_ref, up_sum_ref, total_ref):
+def own_kernel(own_ref, gain_ref, gate_ref, up_ref, _, gate_sum_ref, up_sum_ref, total_ref):
     rows, total, part = scaled_half(own_ref, gain_ref, lax.axis_index("tp"))
     total_ref[...] = jnp.broadcast_to(total, total_ref.shape)
     hidden = gate_ref.shape[1]
@@ -368,12 +381,28 @@
     other = across(residual)
     far_residual = opposite(residual)
     (head,) = call(head_kernel, [((8, 128), f32)], HEAD_FLOPS)()
-    operands = (
+    groups, width = decay_rate.shape
+    per_group = input_map.shape[3]
+    count = max(1, min(groups, 128 // per_group))
+    bars, tables = call(
+        prepare_kernel,
+        [
+            ((2, groups * width), f32),
+            ((groups // count, 6, count * per_group, count * width), bf16),
+        ],
+        10**6,
+        PREPARE_VMEM,
+    )(
         decay_rate,
         frequency,
         step_size.reshape(1, -1),
         jnp.swapaxes(input_map, 2, 3),
         output_matrix,
+        head,
+    )
+    operands = (
+        bars,
+        tables,
         residual,
         other,
         mix_gain.reshape(1, -1),
@@ -382,7 +411,6 @@
         route_ids.T,
         route_weights.T,
         carried_state,
-        head,
     )
     active, new_state = call(
         mixer_kernel,
@@ -391,6 +419,7 @@
         MIXER_VMEM,
     )(*operands)
     far_active = opposite(active)
+    (new_state,) = call(store_kernel, [(new_state.shape, f32)], 10**6)(new_state)
     mid, high, low, far_high, far_low, *sent = call(
         functools.partial(dispatch_kernel, span, top),
         [((rows, half), bf16)]
@@ -418,7 +447,7 @@
             own_kernel,
             [((share, hidden), f32)] * 2 + [((share, 128), f32)],
             4 * share * half * hidden,
-        )(packed, gain, gate, up)
+        )(packed, gain, gate, up, down)
         state, send = call(
             expert_kernel,
             [((share, hidden), bf16), ((share, half), bf16)],

time: 79 us -> 77.2 us (0.977)
  waiting for transfers between devices: 26 us -> 23.7 us
  Pallas kernels: 11.8 us -> 12.7 us
    pallas_call x0 -> x2, Pallas kernels: none -> 1.76 us  [the longest x1 1.04 us: local(): call(store_kernel, [(new_state.shape, f32)], 10 ** 6)(new_state)]
    ppermute x7, waiting for transfers between devices: 1.6 us -> 0.41 us  [across(): return lax.ppermute(values, 'tp', [(0, 1), (1, 0)])]
    ppermute x14, waiting for transfers between devices: 14.9 us -> 13.9 us  [within(): return lax.ppermute(values, 'ep', [(e, e ^ t) for e in range(peers)])]
    pallas_call x1, Pallas kernels: 2.62 us -> 1.73 us  [local(): call(mixer_kernel, [((rows + 8, channel_half), bf16), (carried_state.shap...]
  transfers between devices with their start and end apart: 24 -> 24, of which waited for: 12 -> 10; matrix products, arithmetic and copies ran while one was open for 0% -> 0% of each run, Pallas kernels for 9% -> 11%
where the time goes in v2:
time: 77.2 us; the launch traced here: 77 us
  starting transfers between devices  27.4 us (35%)
  waiting for transfers between devices  23.7 us (31%)
  Pallas kernels  12.7 us (16%)
  blocking collectives  11.2 us (15%)
  local copies, waits for them, and re-layouts  1.07 us (1%)
  between operations  0.98 us (1%)
    ppermute x14, starting transfers between devices, within(): return lax.ppermute(values, 'ep', [(e, e ^ t) for e in range(peers)])  18.6 us
    ppermute x14, waiting for transfers between devices, within(): return lax.ppermute(values, 'ep', [(e, e ^ t) for e in range(peers)])  13.9 us
    all_to_all x1, blocking collectives, returned(): lax.all_to_all(values, 'ep', split_axis=0, concat_axis=0, tiled=True, axi...  11.2 us
    ppermute x3, waiting for transfers between devices, opposite(): return lax.ppermute(values, 'ep', [(e, e ^ inner) for e in range(peers)])  9.45 us
    ppermute x3, starting transfers between devices, opposite(): return lax.ppermute(values, 'ep', [(e, e ^ inner) for e in range(peers)])  7.47 us
    pallas_call x2, Pallas kernels, local(): call(expert_kernel, [((share, hidden), bf16), ((share, half), bf16)], 6 *...  3.46 us
    pallas_call x2, Pallas kernels, local(): call(own_kernel, [((share, hidden), f32)] * 2 + [((share, 128), f32)], 4...  2.03 us
    pallas_call x1, Pallas kernels, local(): call(mixer_kernel, [((rows + 8, channel_half), bf16), (carried_state.shap...  1.73 us
  transfers between devices with their start and end apart: 24, of which 10 were waited for; matrix products, arithmetic and copies ran while one was open for 0% of the time, Pallas kernels for 11%

profile of v2, /device:TPU:0, one launch (start us, length us, event | category | flops | bytes accessed | tf_op | source)
XLA Modules:
  0.0 77.0 jit_solution(11873215004006667749)
XLA Ops:
  0.8 0.6 collective-permute-start
  1.3 0.4 copy-done.6
  1.7 0.2 copy-done.5
  1.9 0.7 shard_map.186
  2.6 0.0 collective-permute-done.refs_3_
  2.7 0.2 copy-done.3
  2.8 0.3 copy-done.4
  3.1 1.7 %shard_map.187 = (bf16[72,512]{1,0:T(8,128)(2,1)S(1)}, f32[2,64,2048]{2,1,0:T(8,128)S(1)}) custom-call(f32[2,2048]{1,0:T(2,128)S(1)} %get-tuple-element.38.refs_0_, bf16[4,6,128,512]{3,2,1,0:T(8,128)(2,1)S(1)} %get-tuple-element.39.refs_1_, bf16[64,1024]{1,0:T(8,128)(2,1)S(1)} %copy-done.7, bf16[64,1024]{1,0:T(8,128)(2,1)S(1)} %collective-permute-done.refs_3_, ...), custom_call_target="tpu_custom_call" | custom-call | flops 1000000000 | bytes 1000000 | tf_op jit(solution)/shard_map/pallas_call | solution.py:415
  4.8 4.1 %collective-permute-start.2 = (bf16[72,512]{1,0:T(8,128)(2,1)S(1)}, bf16[72,512]{1,0:T(8,128)(2,1)S(1)}, u32[]{:S(2)}, u32[]{:S(2)}) collective-permute-start(bf16[72,512]{1,0:T(8,128)(2,1)S(1)} %get-tuple-element.40.own_ref), channel_id=1, source_target_pairs={{0,16},{2,18},{4,20},{6,22},{8,24},{10,26},{12,28},{14,30},{16,0},... | collective-permute-start | bytes 221192 | tf_op jit(solution)/shard_map/ppermute | solution.py:368
  9.0 0.1 collective-permute-start.4
  9.0 6.9 %collective-permute-done.2.far_own_ref = bf16[72,512]{1,0:T(8,128)(2,1)S(1)} collective-permute-done((bf16[72,512]{1,0:T(8,128)(2,1)S(1)}, bf16[72,512]{1,0:T(8,128)(2,1)S(1)}, u32[]{:S(2)}, u32[]{:S(2)}) %collective-permute-start.2) | collective-permute-done | bytes 73760 | tf_op jit(solution)/shard_map/ppermute | solution.py:368
  15.9 0.0 collective-permute-start.3
  15.9 2.6 %collective-permute-done.4.far_residual_ref = bf16[64,1024]{1,0:T(8,128)(2,1)S(1)} collective-permute-done((bf16[64,1024]{1,0:T(8,128)(2,1)S(1)}, bf16[64,1024]{1,0:T(8,128)(2,1)S(1)}, u32[]{:S(2)}, u32[]{:S(2)}) %collective-permute-start.4) | collective-permute-done | bytes 131104 | tf_op jit(solution)/shard_map/ppermute | solution.py:368
  18.5 0.0 collective-permute-done.1.other_ref
  18.5 0.0 collective-permute-done.3.far_other_ref
  18.5 0.0 copy-start
  18.5 0.0 copy-start.1
  18.5 0.0 copy-start.2
  18.6 0.0 copy-start.8
  18.6 1.0 %shard_map.188 = (bf16[64,1024]{1,0:T(8,128)(2,1)S(1)}, bf16[192,64]{1,0:T(8,128)(2,1)S(1)}, bf16[192,64]{1,0:T(8,128)(2,1)S(1)}, bf16[192,64]{1,0:T(8,128)(2,1)...) custom-call(bf16[72,512]{1,0:T(8,128)(2,1)S(1)} %get-tuple-element.4, ...), custom_call_target="tpu_custom_call" | custom-call | flops 10000000000 | bytes 1000000 | tf_op jit(solution)/shard_map/pallas_call | solution.py:423
  19.5 0.7 collective-permute-start.10
  20.3 2.5 %collective-permute-start.11 = (bf16[48,1024]{1,0:T(8,128)(2,1)S(1)}, bf16[48,1024]{1,0:T(8,128)(2,1)S(1)}, u32[]{:S(2)}, u32[]{:S(2)}) collective-permute-start(bf16[48,1024]{1,0:T(8,128)(2,1)S(1)} %get-tuple-element.56), channel_id=1, source_target_pairs={{0,10},{2,8},{4,14},{6,12},{8,2},{10,0},{12,6},{14,4},{16,26},{18,... | collective-permute-start | bytes 294920 | tf_op jit(solution)/shard_map/ppermute | solution.py:371
  22.8 1.4 %collective-permute-start.12 = (bf16[48,1024]{1,0:T(8,128)(2,1)S(1)}, bf16[48,1024]{1,0:T(8,128)(2,1)S(1)}, u32[]{:S(2)}, u32[]{:S(2)}) collective-permute-start(bf16[48,1024]{1,0:T(8,128)(2,1)S(1)} %get-tuple-element.57), channel_id=1, source_target_pairs={{0,12},{2,14},{4,8},{6,10},{8,4},{10,6},{12,0},{14,2},{16,28},{18,... | collective-permute-start | bytes 294920 | tf_op jit(solution)/shard_map/ppermute | solution.py:371
  24.2 1.3 %collective-permute-start.13 = (bf16[48,1024]{1,0:T(8,128)(2,1)S(1)}, bf16[48,1024]{1,0:T(8,128)(2,1)S(1)}, u32[]{:S(2)}, u32[]{:S(2)}) collective-permute-start(bf16[48,1024]{1,0:T(8,128)(2,1)S(1)} %get-tuple-element.58), channel_id=1, source_target_pairs={{0,14},{2,12},{4,10},{6,8},{8,6},{10,4},{12,2},{14,0},{16,30},{18,... | collective-permute-start | bytes 294920 | tf_op jit(solution)/shard_map/ppermute | solution.py:371
  25.5 0.0 collective-permute-done.10.refs_0_
  25.5 3.1 %collective-permute-done.11.refs_1_ = bf16[48,1024]{1,0:T(8,128)(2,1)S(1)} collective-permute-done((bf16[48,1024]{1,0:T(8,128)(2,1)S(1)}, bf16[48,1024]{1,0:T(8,128)(2,1)S(1)}, u32[]{:S(2)}, u32[]{:S(2)}) %collective-permute-start.11) | collective-permute-done | bytes 98336 | tf_op jit(solution)/shard_map/ppermute | solution.py:371
  28.5 2.0 %collective-permute-done.12.refs_2_ = bf16[48,1024]{1,0:T(8,128)(2,1)S(1)} collective-permute-done((bf16[48,1024]{1,0:T(8,128)(2,1)S(1)}, bf16[48,1024]{1,0:T(8,128)(2,1)S(1)}, u32[]{:S(2)}, u32[]{:S(2)}) %collective-permute-start.12) | collective-permute-done | bytes 98336 | tf_op jit(solution)/shard_map/ppermute | solution.py:371
  30.5 1.9 %collective-permute-done.13.refs_3_ = bf16[48,1024]{1,0:T(8,128)(2,1)S(1)} collective-permute-done((bf16[48,1024]{1,0:T(8,128)(2,1)S(1)}, bf16[48,1024]{1,0:T(8,128)(2,1)S(1)}, u32[]{:S(2)}, u32[]{:S(2)}) %collective-permute-start.13) | collective-permute-done | bytes 98336 | tf_op jit(solution)/shard_map/ppermute | solution.py:371
  32.4 0.1 collective-permute-start.14
  32.5 0.9 %collective-permute-start.5 = (bf16[48,1024]{1,0:T(8,128)(2,1)S(1)}, bf16[48,1024]{1,0:T(8,128)(2,1)S(1)}, u32[]{:S(2)}, u32[]{:S(2)}) collective-permute-start(bf16[48,1024]{1,0:T(8,128)(2,1)S(1)} %get-tuple-element.47), channel_id=1, source_target_pairs={{0,2},{2,0},{4,6},{6,4},{8,10},{10,8},{12,14},{14,12},{16,18},{18,... | collective-permute-start | bytes 294920 | tf_op jit(solution)/shard_map/ppermute | solution.py:371
  33.4 0.4 collective-permute-start.6
  33.8 2.2 %collective-permute-start.7 = (bf16[48,1024]{1,0:T(8,128)(2,1)S(1)}, bf16[48,1024]{1,0:T(8,128)(2,1)S(1)}, u32[]{:S(2)}, u32[]{:S(2)}) collective-permute-start(bf16[48,1024]{1,0:T(8,128)(2,1)S(1)} %get-tuple-element.49), channel_id=1, source_target_pairs={{0,6},{2,4},{4,2},{6,0},{8,14},{10,12},{12,10},{14,8},{16,22},{18,... | collective-permute-start | bytes 294920 | tf_op jit(solution)/shard_map/ppermute | solution.py:371
  36.1 2.0 %collective-permute-done.5.refs_1_ = bf16[48,1024]{1,0:T(8,128)(2,1)S(1)} collective-permute-done((bf16[48,1024]{1,0:T(8,128)(2,1)S(1)}, bf16[48,1024]{1,0:T(8,128)(2,1)S(1)}, u32[]{:S(2)}, u32[]{:S(2)}) %collective-permute-start.5) | collective-permute-done | bytes 98336 | tf_op jit(solution)/shard_map/ppermute | solution.py:371
  38.0 2.4 %collective-permute-done.6.refs_2_ = bf16[48,1024]{1,0:T(8,128)(2,1)S(1)} collective-permute-done((bf16[48,1024]{1,0:T(8,128)(2,1)S(1)}, bf16[48,1024]{1,0:T(8,128)(2,1)S(1)}, u32[]{:S(2)}, u32[]{:S(2)}) %collective-permute-start.6) | collective-permute-done | bytes 98336 | tf_op jit(solution)/shard_map/ppermute | solution.py:371
  40.4 0.0 collective-permute-done.7.refs_3_
  40.4 0.1 collective-permute-start.8
  40.5 1.0 %shard_map.194 = (f32[192,1024]{1,0:T(8,128)S(1)}, f32[192,1024]{1,0:T(8,128)S(1)}, f32[192,128]{1,0:T(8,128)S(1)}) custom-call(bf16[192,1024]{1,0:T(8,128)(2,1)S(1)} %shard_map.193.own_ref, f32[1,2048]{1,0:T(1,128)S(1)} %bitcast.28, bf16[2048,1024]{1,0:T(8,128)(2,1)S(1)} %bitcast.18, bf16[2048,1024]{1,0:T(8,128)(2,1)S(1)} %bitcast.22, ...), custom_call_target="tpu_custom_call" | custom-call | flops 805306368 | bytes 1000000 | tf_op jit(solution)/shard_map/pallas_call | solution.py:446
  41.6 1.0 %shard_map.190 = (f32[192,1024]{1,0:T(8,128)S(1)}, f32[192,1024]{1,0:T(8,128)S(1)}, f32[192,128]{1,0:T(8,128)S(1)}) custom-call(bf16[192,1024]{1,0:T(8,128)(2,1)S(1)} %shard_map.189.own_ref, f32[1,2048]{1,0:T(1,128)S(1)} %bitcast.29, bf16[2048,1024]{1,0:T(8,128)(2,1)S(1)} %bitcast.19, bf16[2048,1024]{1,0:T(8,128)(2,1)S(1)} %bitcast.23, ...), custom_call_target="tpu_custom_call" | custom-call | flops 805306368 | bytes 1000000 | tf_op jit(solution)/shard_map/pallas_call | solution.py:446
  42.6 1.7 %shard_map.195 = (bf16[192,1024]{1,0:T(8,128)(2,1)S(1)}, bf16[192,1024]{1,0:T(8,128)(2,1)S(1)}) custom-call(bf16[192,1024]{1,0:T(8,128)(2,1)S(1)} %collective-permute-done.14.other_ref, f32[192,1024]{1,0:T(8,128)S(1)} %get-tuple-element.59.gate_sum_ref, f32[192,1024]{1,0:T(8,128)S(1)} %get-tuple-element.60.up_sum_ref, ...), custom_call_target="tpu_custom_call" | custom-call | flops 1207959552 | bytes 1000000 | tf_op jit(solution)/shard_map/pallas_call | solution.py:451
  44.3 0.5 collective-permute-start.15
  44.9 0.0 collective-permute-done.8.other_ref
  44.9 1.7 %shard_map.191 = (bf16[192,1024]{1,0:T(8,128)(2,1)S(1)}, bf16[192,1024]{1,0:T(8,128)(2,1)S(1)}) custom-call(bf16[192,1024]{1,0:T(8,128)(2,1)S(1)} %collective-permute-done.8.other_ref, f32[192,1024]{1,0:T(8,128)S(1)} %get-tuple-element.50.gate_sum_ref, f32[192,1024]{1,0:T(8,128)S(1)} %get-tuple-element.51.up_sum_ref, ...), custom_call_target="tpu_custom_call" | custom-call | flops 1207959552 | bytes 1000000 | tf_op jit(solution)/shard_map/pallas_call | solution.py:451
  46.6 0.1 collective-permute-start.9
  46.7 0.6 shard_map.196.refs_2_
  47.4 0.6 shard_map.192.refs_0_
  48.0 0.0 collective-permute-done.15.refs_3_
  48.0 0.4 collective-permute-done.9.refs_1_
  48.4 0.2 shard_map.197
  48.6 11.2 %all_to_all.5 = bf16[8,24,1024]{2,1,0:T(8,128)(2,1)S(1)} all-to-all(bf16[8,24,1024]{2,1,0:T(8,128)(2,1)S(1)} %get-tuple-element.64), channel_id=1, replica_groups={{0,2,4,6,8,10,12,14},{16,18,20,22,24,26,28,30},{1,3,5,7,9,11,13,15},{17..., dimensions={0} | all-to-all | bytes 786432 | tf_op jit(solution)/shard_map/all_to_all | solution.py:376
  59.8 0.3 shard_map.198
  60.1 3.3 %collective-permute-start.16 = (bf16[64,1024]{1,0:T(8,128)(2,1)S(1)}, bf16[64,1024]{1,0:T(8,128)(2,1)S(1)}, u32[]{:S(2)}, u32[]{:S(2)}) collective-permute-start(bf16[64,1024]{1,0:T(8,128)(2,1)S(1)} %shard_map.198), channel_id=1, source_target_pairs={{0,16},{2,18},{4,20},{6,22},{8,24},{10,26},{12,28},{14,30},{16,0},... | collective-permute-start | bytes 393224 | tf_op jit(solution)/shard_map/ppermute | solution.py:368
  63.3 0.4 collective-permute-start.17
  63.7 0.9 %collective-permute-start.18 = (bf16[24,1024]{1,0:T(8,128)(2,1)S(1)}, bf16[24,1024]{1,0:T(8,128)(2,1)S(1)}, u32[]{:S(2)}, u32[]{:S(2)}) collective-permute-start(bf16[24,1024]{1,0:T(8,128)(2,1)S(1)} %get-tuple-element.67), channel_id=1, source_target_pairs={{0,4},{2,6},{4,0},{6,2},{8,12},{10,14},{12,8},{14,10},{16,20},{18,... | collective-permute-start | bytes 147464 | tf_op jit(solution)/shard_map/ppermute | solution.py:371
  64.6 2.2 %collective-permute-start.19 = (bf16[24,1024]{1,0:T(8,128)(2,1)S(1)}, bf16[24,1024]{1,0:T(8,128)(2,1)S(1)}, u32[]{:S(2)}, u32[]{:S(2)}) collective-permute-start(bf16[24,1024]{1,0:T(8,128)(2,1)S(1)} %get-tuple-element.68), channel_id=1, source_target_pairs={{0,6},{2,4},{4,2},{6,0},{8,14},{10,12},{12,10},{14,8},{16,22},{18,... | collective-permute-start | bytes 147464 | tf_op jit(solution)/shard_map/ppermute | solution.py:371
  66.8 0.7 collective-permute-start.20
  67.5 1.1 %collective-permute-start.21 = (bf16[24,1024]{1,0:T(8,128)(2,1)S(1)}, bf16[24,1024]{1,0:T(8,128)(2,1)S(1)}, u32[]{:S(2)}, u32[]{:S(2)}) collective-permute-start(bf16[24,1024]{1,0:T(8,128)(2,1)S(1)} %get-tuple-element.70), channel_id=1, source_target_pairs={{0,10},{2,8},{4,14},{6,12},{8,2},{10,0},{12,6},{14,4},{16,26},{18,... | collective-permute-start | bytes 147464 | tf_op jit(solution)/shard_map/ppermute | solution.py:371
  68.7 1.2 %collective-permute-start.22 = (bf16[24,1024]{1,0:T(8,128)(2,1)S(1)}, bf16[24,1024]{1,0:T(8,128)(2,1)S(1)}, u32[]{:S(2)}, u32[]{:S(2)}) collective-permute-start(bf16[24,1024]{1,0:T(8,128)(2,1)S(1)} %get-tuple-element.71), channel_id=1, source_target_pairs={{0,12},{2,14},{4,8},{6,10},{8,4},{10,6},{12,0},{14,2},{16,28},{18,... | collective-permute-start | bytes 147464 | tf_op jit(solution)/shard_map/ppermute | solution.py:371
  69.9 0.3 collective-permute-done.19.refs_3_
  70.2 2.5 %collective-permute-start.23 = (bf16[24,1024]{1,0:T(8,128)(2,1)S(1)}, bf16[24,1024]{1,0:T(8,128)(2,1)S(1)}, u32[]{:S(2)}, u32[]{:S(2)}) collective-permute-start(bf16[24,1024]{1,0:T(8,128)(2,1)S(1)} %get-tuple-element.72), channel_id=1, source_target_pairs={{0,14},{2,12},{4,10},{6,8},{8,6},{10,4},{12,2},{14,0},{16,30},{18,... | collective-permute-start | bytes 147464 | tf_op jit(solution)/shard_map/ppermute | solution.py:371
  72.7 1.0 %shard_map.200 = f32[2,64,2048]{2,1,0:T(8,128)} custom-call(f32[2,64,2048]{2,1,0:T(8,128)S(1)} %get-tuple-element.73.value_ref), custom_call_target="tpu_custom_call" | custom-call | flops 1000000 | bytes 1000000 | tf_op jit(solution)/shard_map/pallas_call | solution.py:422
  73.7 0.0 collective-permute-done.22.refs_6_
  73.7 2.3 %collective-permute-done.23.refs_7_ = bf16[24,1024]{1,0:T(8,128)(2,1)S(1)} collective-permute-done((bf16[24,1024]{1,0:T(8,128)(2,1)S(1)}, bf16[24,1024]{1,0:T(8,128)(2,1)S(1)}, u32[]{:S(2)}, u32[]{:S(2)}) %collective-permute-start.23) | collective-permute-done | bytes 49184 | tf_op jit(solution)/shard_map/ppermute | solution.py:371
  76.0 0.0 collective-permute-done.16.far_ref
  76.0 0.9 %shard_map.199 = bf16[64,1024]{1,0:T(8,128)(2,1)} custom-call(bf16[192,64]{1,0:T(8,128)(2,1)S(1)} %get-tuple-element.41.high_ref, bf16[192,64]{1,0:T(8,128)(2,1)S(1)} %get-tuple-element.42.low_ref, bf16[64,1024]{1,0:T(8,128)(2,1)S(1)} %get-tuple-element.43.mid_ref, bf16[64,1024]{1,0:T(8,128)(2,1)S(1)} %collective-permute-done.16.far_ref, ...), custom_call_target="tpu_custom_call" | custom-call | flops 1000000 | bytes 1000000 | tf_op jit(solution)/shard_map/pallas_call | solution.py:466
  (37 shorter events, 0.1 us)
Async XLA Ops:
  0.6 2.0 %copy-start.7 = (bf16[64,1024]{1,0:T(8,128)(2,1)S(1)}, bf16[64,1024]{1,0:T(8,128)(2,1)}, u32[]{:S(2)}) copy-start(bf16[64,1024]{1,0:T(8,128)(2,1)} %residual_ref.1) | copy-start | bytes 393220
  0.6 1.1 %copy-start.6 = (f32[2,32,16,64]{3,2,1,0:T(8,128)S(1)}, f32[2,32,16,64]{3,2,1,0:T(8,128)}, u32[]{:S(2)}) copy-start(f32[2,32,16,64]{3,2,1,0:T(8,128)} %out_ref.1) | copy-start | bytes 786436
  0.7 1.2 %copy-start.5 = (f32[2,32,64,16]{2,3,1,0:T(8,128)S(1)}, f32[2,32,64,16]{2,3,1,0:T(8,128)}, u32[]{:S(2)}) copy-start(f32[2,32,64,16]{2,3,1,0:T(8,128)} %param.27) | copy-start | bytes 786436
  0.7 1.2 %copy-start.15 = (f32[32]{0:T(128)S(1)}, f32[32]{0:T(128)}, u32[]{:S(2)}) copy-start(f32[32]{0:T(128)} %param.26) | copy-start | bytes 388
  0.7 1.2 %copy-start.10 = (f32[32,64]{1,0:T(8,128)S(1)}, f32[32,64]{1,0:T(8,128)}, u32[]{:S(2)}) copy-start(f32[32,64]{1,0:T(8,128)} %freq_ref.1) | copy-start | bytes 24580
  0.7 1.2 %copy-start.9 = (f32[32,64]{1,0:T(8,128)S(1)}, f32[32,64]{1,0:T(8,128)}, u32[]{:S(2)}) copy-start(f32[32,64]{1,0:T(8,128)} %decay_ref.1) | copy-start | bytes 24580
  0.7 1.9 %copy-start.12 = (f32[512]{0:T(512)S(1)}, f32[512]{0:T(512)}, u32[]{:S(2)}) copy-start(f32[512]{0:T(512)} %param.29) | copy-start | bytes 6148
  0.7 2.1 %copy-start.3 = (bf16[2048,512]{1,0:T(8,128)(2,1)S(1)}, bf16[2048,512]{1,0:T(8,128)(2,1)}, u32[]{:S(2)}) copy-start(bf16[2048,512]{1,0:T(8,128)(2,1)} %refs_5_.1) | copy-start | bytes 6291460
  0.7 2.1 %copy-start.11 = (f32[2048]{0:T(1024)S(1)}, f32[2048]{0:T(1024)}, u32[]{:S(2)}) copy-start(f32[2048]{0:T(1024)} %param.22) | copy-start | bytes 24580
  0.7 2.4 %copy-start.4 = (f32[2,64,2048]{2,1,0:T(8,128)S(1)}, f32[2,64,2048]{2,1,0:T(8,128)}, u32[]{:S(2)}) copy-start(f32[2,64,2048]{2,1,0:T(8,128)} %refs_9_.1) | copy-start | bytes 3145732
  0.7 2.4 %copy-start.14 = (f32[64,4]{0,1:T(4,128)S(1)}, f32[64,4]{0,1:T(4,128)}, u32[]{:S(2)}) copy-start(f32[64,4]{0,1:T(4,128)} %param.20) | copy-start | bytes 3076
  0.7 2.3 %copy-start.13 = (s32[64,4]{0,1:T(4,128)S(1)}, s32[64,4]{0,1:T(4,128)}, u32[]{:S(2)}) copy-start(s32[64,4]{0,1:T(4,128)} %param.19) | copy-start | bytes 3076
  0.8 1.9 %collective-permute-start = (bf16[64,1024]{1,0:T(8,128)(2,1)}, bf16[64,1024]{1,0:T(8,128)(2,1)S(1)}, u32[]{:S(2)}, u32[]{:S(2)}) collective-permute-start(bf16[64,1024]{1,0:T(8,128)(2,1)} %residual_ref.1), channel_id=1, source_target_pairs={{0,1},{1,0},{2,3},{3,2},{4,5},{5,4},{6,7},{7,6},{8,9},{9,8},{10,11... | collective-permute-start | bytes 393224 | tf_op jit(solution)/shard_map/ppermute | solution.py:365
  1.3 17.2 %copy-start.16 = (bf16[1024,1024]{1,0:T(8,128)(2,1)S(1)}, bf16[1024,1024]{1,0:T(8,128)(2,1)}, u32[]{:S(2)}) copy-start(bf16[1024,1024]{1,0:T(8,128)(2,1)} %proj_ref.1) | copy-start | bytes 6291460
  1.3 17.2 %copy-start.17 = (f32[1024]{0:T(1024)S(1)}, f32[1024]{0:T(1024)}, u32[]{:S(2)}) copy-start(f32[1024]{0:T(1024)} %param.30) | copy-start | bytes 12292
  4.8 11.1 %collective-permute-start.2 = (bf16[72,512]{1,0:T(8,128)(2,1)S(1)}, bf16[72,512]{1,0:T(8,128)(2,1)S(1)}, u32[]{:S(2)}, u32[]{:S(2)}) collective-permute-start(bf16[72,512]{1,0:T(8,128)(2,1)S(1)} %get-tuple-element.40.own_ref), channel_id=1, source_target_pairs={{0,16},{2,18},{4,20},{6,22},{8,24},{10,26},{12,28},{14,30},{16,0},... | collective-permute-start | bytes 221192 | tf_op jit(solution)/shard_map/ppermute | solution.py:368
  9.0 9.5 %collective-permute-start.4 = (bf16[64,1024]{1,0:T(8,128)(2,1)S(1)}, bf16[64,1024]{1,0:T(8,128)(2,1)S(1)}, u32[]{:S(2)}, u32[]{:S(2)}) collective-permute-start(bf16[64,1024]{1,0:T(8,128)(2,1)S(1)} %copy-done.7), channel_id=1, source_target_pairs={{0,16},{2,18},{4,20},{6,22},{8,24},{10,26},{12,28},{14,30},{16,0},... | collective-permute-start | bytes 393224 | tf_op jit(solution)/shard_map/ppermute | solution.py:368
  9.0 9.5 %collective-permute-start.1 = (bf16[72,512]{1,0:T(8,128)(2,1)S(1)}, bf16[72,512]{1,0:T(8,128)(2,1)S(1)}, u32[]{:S(2)}, u32[]{:S(2)}) collective-permute-start(bf16[72,512]{1,0:T(8,128)(2,1)S(1)} %get-tuple-element.40.own_ref), channel_id=1, source_target_pairs={{0,1},{1,0},{2,3},{3,2},{4,5},{5,4},{6,7},{7,6},{8,9},{9,8},{10,11... | collective-permute-start | bytes 221192 | tf_op jit(solution)/shard_map/ppermute | solution.py:365
  15.9 2.6 %collective-permute-start.3 = (bf16[72,512]{1,0:T(8,128)(2,1)S(1)}, bf16[72,512]{1,0:T(8,128)(2,1)S(1)}, u32[]{:S(2)}, u32[]{:S(2)}) collective-permute-start(bf16[72,512]{1,0:T(8,128)(2,1)S(1)} %collective-permute-done.2.far_own_ref), channel_id=1, source_target_pairs={{0,1},{1,0},{2,3},{3,2},{4,5},{5,4},{6,7},{7,6},{8,9},{9,8},{10,11... | collective-permute-start | bytes 221192 | tf_op jit(solution)/shard_map/ppermute | solution.py:365
  18.5 22.0 %copy-start = (bf16[1,1024,2048]{2,1,0:T(8,128)(2,1)S(1)}, bf16[1,1024,2048]{2,1,0:T(8,128)(2,1)}, u32[]{:S(2)}) copy-start(bf16[1,1024,2048]{2,1,0:T(8,128)(2,1)} %param.35) | copy-start | bytes 12582916
  18.5 22.0 %copy-start.1 = (bf16[1,2048,1024]{2,1,0:T(8,128)(2,1)S(1)}, bf16[1,2048,1024]{2,1,0:T(8,128)(2,1)}, u32[]{:S(2)}) copy-start(bf16[1,2048,1024]{2,1,0:T(8,128)(2,1)} %param.33) | copy-start | bytes 12582916
  18.5 22.0 %copy-start.2 = (bf16[1,2048,1024]{2,1,0:T(8,128)(2,1)S(1)}, bf16[1,2048,1024]{2,1,0:T(8,128)(2,1)}, u32[]{:S(2)}) copy-start(bf16[1,2048,1024]{2,1,0:T(8,128)(2,1)} %param.34) | copy-start | bytes 12582916
  18.6 22.0 %copy-start.8 = (f32[2048]{0:T(1024)S(1)}, f32[2048]{0:T(1024)}, u32[]{:S(2)}) copy-start(f32[2048]{0:T(1024)} %param.32) | copy-start | bytes 24580
  19.5 5.9 %collective-permute-start.10 = (bf16[48,1024]{1,0:T(8,128)(2,1)S(1)}, bf16[48,1024]{1,0:T(8,128)(2,1)S(1)}, u32[]{:S(2)}, u32[]{:S(2)}) collective-permute-start(bf16[48,1024]{1,0:T(8,128)(2,1)S(1)} %get-tuple-element.55), channel_id=1, source_target_pairs={{0,8},{2,10},{4,12},{6,14},{8,0},{10,2},{12,4},{14,6},{16,24},{18,... | collective-permute-start | bytes 294920 | tf_op jit(solution)/shard_map/ppermute | solution.py:371
  20.3 8.3 %collective-permute-start.11 = (bf16[48,1024]{1,0:T(8,128)(2,1)S(1)}, bf16[48,1024]{1,0:T(8,128)(2,1)S(1)}, u32[]{:S(2)}, u32[]{:S(2)}) collective-permute-start(bf16[48,1024]{1,0:T(8,128)(2,1)S(1)} %get-tuple-element.56), channel_id=1, source_target_pairs={{0,10},{2,8},{4,14},{6,12},{8,2},{10,0},{12,6},{14,4},{16,26},{18,... | collective-permute-start | bytes 294920 | tf_op jit(solution)/shard_map/ppermute | solution.py:371
  22.8 7.7 %collective-permute-start.12 = (bf16[48,1024]{1,0:T(8,128)(2,1)S(1)}, bf16[48,1024]{1,0:T(8,128)(2,1)S(1)}, u32[]{:S(2)}, u32[]{:S(2)}) collective-permute-start(bf16[48,1024]{1,0:T(8,128)(2,1)S(1)} %get-tuple-element.57), channel_id=1, source_target_pairs={{0,12},{2,14},{4,8},{6,10},{8,4},{10,6},{12,0},{14,2},{16,28},{18,... | collective-permute-start | bytes 294920 | tf_op jit(solution)/shard_map/ppermute | solution.py:371
  24.2 8.2 %collective-permute-start.13 = (bf16[48,1024]{1,0:T(8,128)(2,1)S(1)}, bf16[48,1024]{1,0:T(8,128)(2,1)S(1)}, u32[]{:S(2)}, u32[]{:S(2)}) collective-permute-start(bf16[48,1024]{1,0:T(8,128)(2,1)S(1)} %get-tuple-element.58), channel_id=1, source_target_pairs={{0,14},{2,12},{4,10},{6,8},{8,6},{10,4},{12,2},{14,0},{16,30},{18,... | collective-permute-start | bytes 294920 | tf_op jit(solution)/shard_map/ppermute | solution.py:371
  32.4 10.2 %collective-permute-start.14 = (bf16[192,1024]{1,0:T(8,128)(2,1)S(1)}, bf16[192,1024]{1,0:T(8,128)(2,1)S(1)}, u32[]{:S(2)}, u32[]{:S(2)}) collective-permute-start(bf16[192,1024]{1,0:T(8,128)(2,1)S(1)} %shard_map.193.own_ref), channel_id=1, source_target_pairs={{0,1},{1,0},{2,3},{3,2},{4,5},{5,4},{6,7},{7,6},{8,9},{9,8},{10,11... | collective-permute-start | bytes 1179656 | tf_op jit(solution)/shard_map/ppermute | solution.py:365
  32.5 5.5 %collective-permute-start.5 = (bf16[48,1024]{1,0:T(8,128)(2,1)S(1)}, bf16[48,1024]{1,0:T(8,128)(2,1)S(1)}, u32[]{:S(2)}, u32[]{:S(2)}) collective-permute-start(bf16[48,1024]{1,0:T(8,128)(2,1)S(1)} %get-tuple-element.47), channel_id=1, source_target_pairs={{0,2},{2,0},{4,6},{6,4},{8,10},{10,8},{12,14},{14,12},{16,18},{18,... | collective-permute-start | bytes 294920 | tf_op jit(solution)/shard_map/ppermute | solution.py:371
  33.4 7.0 %collective-permute-start.6 = (bf16[48,1024]{1,0:T(8,128)(2,1)S(1)}, bf16[48,1024]{1,0:T(8,128)(2,1)S(1)}, u32[]{:S(2)}, u32[]{:S(2)}) collective-permute-start(bf16[48,1024]{1,0:T(8,128)(2,1)S(1)} %get-tuple-element.48), channel_id=1, source_target_pairs={{0,4},{2,6},{4,0},{6,2},{8,12},{10,14},{12,8},{14,10},{16,20},{18,... | collective-permute-start | bytes 294920 | tf_op jit(solution)/shard_map/ppermute | solution.py:371
  33.8 6.6 %collective-permute-start.7 = (bf16[48,1024]{1,0:T(8,128)(2,1)S(1)}, bf16[48,1024]{1,0:T(8,128)(2,1)S(1)}, u32[]{:S(2)}, u32[]{:S(2)}) collective-permute-start(bf16[48,1024]{1,0:T(8,128)(2,1)S(1)} %get-tuple-element.49), channel_id=1, source_target_pairs={{0,6},{2,4},{4,2},{6,0},{8,14},{10,12},{12,10},{14,8},{16,22},{18,... | collective-permute-start | bytes 294920 | tf_op jit(solution)/shard_map/ppermute | solution.py:371
  40.4 4.5 %collective-permute-start.8 = (bf16[192,1024]{1,0:T(8,128)(2,1)S(1)}, bf16[192,1024]{1,0:T(8,128)(2,1)S(1)}, u32[]{:S(2)}, u32[]{:S(2)}) collective-permute-start(bf16[192,1024]{1,0:T(8,128)(2,1)S(1)} %shard_map.189.own_ref), channel_id=1, source_target_pairs={{0,1},{1,0},{2,3},{3,2},{4,5},{5,4},{6,7},{7,6},{8,9},{9,8},{10,11... | collective-permute-start | bytes 1179656 | tf_op jit(solution)/shard_map/ppermute | solution.py:365
  44.3 3.7 %collective-permute-start.15 = (bf16[192,1024]{1,0:T(8,128)(2,1)S(1)}, bf16[192,1024]{1,0:T(8,128)(2,1)S(1)}, u32[]{:S(2)}, u32[]{:S(2)}) collective-permute-start(bf16[192,1024]{1,0:T(8,128)(2,1)S(1)} %get-tuple-element.63), channel_id=1, source_target_pairs={{0,1},{1,0},{2,3},{3,2},{4,5},{5,4},{6,7},{7,6},{8,9},{9,8},{10,11... | collective-permute-start | bytes 1179656 | tf_op jit(solution)/shard_map/ppermute | solution.py:365
  46.6 1.8 %collective-permute-start.9 = (bf16[192,1024]{1,0:T(8,128)(2,1)S(1)}, bf16[192,1024]{1,0:T(8,128)(2,1)S(1)}, u32[]{:S(2)}, u32[]{:S(2)}) collective-permute-start(bf16[192,1024]{1,0:T(8,128)(2,1)S(1)} %get-tuple-element.54), channel_id=1, source_target_pairs={{0,1},{1,0},{2,3},{3,2},{4,5},{5,4},{6,7},{7,6},{8,9},{9,8},{10,11... | collective-permute-start | bytes 1179656 | tf_op jit(solution)/shard_map/ppermute | solution.py:365
  60.1 16.0 %collective-permute-start.16 = (bf16[64,1024]{1,0:T(8,128)(2,1)S(1)}, bf16[64,1024]{1,0:T(8,128)(2,1)S(1)}, u32[]{:S(2)}, u32[]{:S(2)}) collective-permute-start(bf16[64,1024]{1,0:T(8,128)(2,1)S(1)} %shard_map.198), channel_id=1, source_target_pairs={{0,16},{2,18},{4,20},{6,22},{8,24},{10,26},{12,28},{14,30},{16,0},... | collective-permute-start | bytes 393224 | tf_op jit(solution)/shard_map/ppermute | solution.py:368
  63.3 4.2 %collective-permute-start.17 = (bf16[24,1024]{1,0:T(8,128)(2,1)S(1)}, bf16[24,1024]{1,0:T(8,128)(2,1)S(1)}, u32[]{:S(2)}, u32[]{:S(2)}) collective-permute-start(bf16[24,1024]{1,0:T(8,128)(2,1)S(1)} %get-tuple-element.66), channel_id=1, source_target_pairs={{0,2},{2,0},{4,6},{6,4},{8,10},{10,8},{12,14},{14,12},{16,18},{18,... | collective-permute-start | bytes 147464 | tf_op jit(solution)/shard_map/ppermute | solution.py:371
  63.7 5.0 %collective-permute-start.18 = (bf16[24,1024]{1,0:T(8,128)(2,1)S(1)}, bf16[24,1024]{1,0:T(8,128)(2,1)S(1)}, u32[]{:S(2)}, u32[]{:S(2)}) collective-permute-start(bf16[24,1024]{1,0:T(8,128)(2,1)S(1)} %get-tuple-element.67), channel_id=1, source_target_pairs={{0,4},{2,6},{4,0},{6,2},{8,12},{10,14},{12,8},{14,10},{16,20},{18,... | collective-permute-start | bytes 147464 | tf_op jit(solution)/shard_map/ppermute | solution.py:371
  64.6 5.5 %collective-permute-start.19 = (bf16[24,1024]{1,0:T(8,128)(2,1)S(1)}, bf16[24,1024]{1,0:T(8,128)(2,1)S(1)}, u32[]{:S(2)}, u32[]{:S(2)}) collective-permute-start(bf16[24,1024]{1,0:T(8,128)(2,1)S(1)} %get-tuple-element.68), channel_id=1, source_target_pairs={{0,6},{2,4},{4,2},{6,0},{8,14},{10,12},{12,10},{14,8},{16,22},{18,... | collective-permute-start | bytes 147464 | tf_op jit(solution)/shard_map/ppermute | solution.py:371
  66.8 6.9 %collective-permute-start.20 = (bf16[24,1024]{1,0:T(8,128)(2,1)S(1)}, bf16[24,1024]{1,0:T(8,128)(2,1)S(1)}, u32[]{:S(2)}, u32[]{:S(2)}) collective-permute-start(bf16[24,1024]{1,0:T(8,128)(2,1)S(1)} %get-tuple-element.69), channel_id=1, source_target_pairs={{0,8},{2,10},{4,12},{6,14},{8,0},{10,2},{12,4},{14,6},{16,24},{18,... | collective-permute-start | bytes 147464 | tf_op jit(solution)/shard_map/ppermute | solution.py:371
  67.5 6.2 %collective-permute-start.21 = (bf16[24,1024]{1,0:T(8,128)(2,1)S(1)}, bf16[24,1024]{1,0:T(8,128)(2,1)S(1)}, u32[]{:S(2)}, u32[]{:S(2)}) collective-permute-start(bf16[24,1024]{1,0:T(8,128)(2,1)S(1)} %get-tuple-element.70), channel_id=1, source_target_pairs={{0,10},{2,8},{4,14},{6,12},{8,2},{10,0},{12,6},{14,4},{16,26},{18,... | collective-permute-start | bytes 147464 | tf_op jit(solution)/shard_map/ppermute | solution.py:371
  68.7 5.1 %collective-permute-start.22 = (bf16[24,1024]{1,0:T(8,128)(2,1)S(1)}, bf16[24,1024]{1,0:T(8,128)(2,1)S(1)}, u32[]{:S(2)}, u32[]{:S(2)}) collective-permute-start(bf16[24,1024]{1,0:T(8,128)(2,1)S(1)} %get-tuple-element.71), channel_id=1, source_target_pairs={{0,12},{2,14},{4,8},{6,10},{8,4},{10,6},{12,0},{14,2},{16,28},{18,... | collective-permute-start | bytes 147464 | tf_op jit(solution)/shard_map/ppermute | solution.py:371
  70.2 5.9 %collective-permute-start.23 = (bf16[24,1024]{1,0:T(8,128)(2,1)S(1)}, bf16[24,1024]{1,0:T(8,128)(2,1)S(1)}, u32[]{:S(2)}, u32[]{:S(2)}) collective-permute-start(bf16[24,1024]{1,0:T(8,128)(2,1)S(1)} %get-tuple-element.72), channel_id=1, source_target_pairs={{0,14},{2,12},{4,10},{6,8},{8,6},{10,4},{12,2},{14,0},{16,30},{18,... | collective-permute-start | bytes 147464 | tf_op jit(solution)/shard_map/ppermute | solution.py:371
